TPU v7x, 32 devices: a whole 2x2x4 slice. The times are simulated.
32 devices in a mesh: sp: 4 (over z), fs: 4 (over y, x), tp: 2 (over core).
Axes of the slice: x: 2, y: 2, z: 4, core: 2. Of those that a mesh axis runs over, the one named last changes fastest.
Arguments:
- tokens: bfloat16 [4, 2048, 2048], P('fs', ('sp', 'tp')), may hold values from -6 to 6
- norm_gain: float32 [2048], replicated, may hold values from 0.1 to 1.9
- query_weight: bfloat16 [2048, 1024], P('sp', 'tp'), may hold values from -20 to 20
- key_matrix: bfloat16 [2048, 256], P('sp', 'tp'), may hold values from -0.125 to 0.125
- value_matrix: bfloat16 [2048, 256], P('sp', 'tp'), may hold values from -0.125 to 0.125
- pool_in_weight: bfloat16 [2048, 1024], P('sp', 'tp'), may hold values from -0.125 to 0.125
- head_sink_logit: float32 [16], replicated, may hold values from 2 to 6
- pool_mix: bfloat16 [4, 256, 256], replicated, may hold values from -0.375 to 0.375
- pool_gain: float32 [1024], replicated, may hold values from 0.1 to 1.9
- attn_out_weight: bfloat16 [1024, 2048], P('tp', 'sp'), may hold values from -1 to 1
- pool_out_weight: bfloat16 [1024, 2048], P('tp', 'sp'), may hold values from -0.125 to 0.125
Outputs:
- mixed: bfloat16 [4, 2048, 2048], P('fs', ('sp', 'tp'))
- row_log_weight_sum: float32 [4, 16, 2048], P('fs', 'tp', 'sp')
All inputs are finite; a program needn't handle non-finite values.
Results may differ from a plain program's by a relative error of at most 0.0095.
The roundings to bfloat16 on the way count: a program that leaves them out, or rounds other values in their place, can miss the bound.
Values may be sent and summed in bfloat16 or wider, within the bound.
A program may use at most 64 MiB of HBM per device.

v0:
```python
import functools

import jax
import jax.numpy as jnp
from jax import lax
from jax.experimental import pallas as pl
from jax.experimental.pallas import tpu as pltpu
from jax.sharding import PartitionSpec as P

HEAD_SIZE = 64
WINDOW = 128
POOL_CH = 256


EPSILON = 1e-06
POOL_SPANS = (2, 4, 8, 16)


def passed_along(shard, axis, by):
    size = lax.axis_size(axis)
    pairs = [(i, i + by) for i in range(size) if 0 <= i + by < size]
    return lax.ppermute(shard, axis, pairs)


def windowed_attend(
    query_rows, key_rows, value_rows, key_tail, value_tail, sinks, kv_heads, group, first_pos
):
    rows = query_rows.shape[0]
    blocks = rows // WINDOW
    width = key_rows.shape[1]
    ext_keys = jnp.concatenate([key_tail, key_rows], 0)
    ext_values = jnp.concatenate([value_tail, value_rows], 0)

    def banded(table):
        return jnp.concatenate(
            [
                table[:rows].reshape(blocks, WINDOW, width),
                table[WINDOW:].reshape(blocks, WINDOW, width),
            ],
            axis=1,
        )

    band_keys = banded(ext_keys).reshape(blocks, 2 * WINDOW, kv_heads, HEAD_SIZE)
    band_values = banded(ext_values).reshape(blocks, 2 * WINDOW, kv_heads, HEAD_SIZE)
    query_blocks = query_rows.reshape(blocks, WINDOW, kv_heads, group, HEAD_SIZE)
    scores = jnp.einsum(
        "bqkgd,bskd->bkgqs", query_blocks, band_keys, preferred_element_type=jnp.float32
    ) * HEAD_SIZE ** (-0.5)
    query_pos = first_pos + jnp.arange(rows).reshape(blocks, WINDOW, 1)
    key_pos = (
        first_pos
        - WINDOW
        + jnp.arange(blocks).reshape(blocks, 1, 1) * WINDOW
        + jnp.arange(2 * WINDOW).reshape(1, 1, 2 * WINDOW)
    )
    offset = query_pos - key_pos
    allowed = (offset >= 0) & (offset < WINDOW) & (key_pos >= 0)
    scores = jnp.where(allowed[:, None, None], scores, -jnp.inf)
    sink_grid = sinks.reshape(1, kv_heads, group, 1, 1)
    top = jnp.maximum(jnp.max(scores, axis=-1, keepdims=True), sink_grid)
    weights = jnp.exp(scores - top)
    total = jnp.sum(weights, axis=-1, keepdims=True) + jnp.exp(sink_grid - top)
    probs = (weights / total).astype(jnp.bfloat16)
    mixed = jnp.einsum(
        "bkgqs,bskd->bqkgd", probs, band_values, preferred_element_type=jnp.float32
    ).astype(jnp.bfloat16)
    row_log_weight_sum = (top + jnp.log(total))[..., 0]
    return (
        mixed.reshape(rows, kv_heads * group * HEAD_SIZE),
        row_log_weight_sum.transpose(1, 2, 0, 3).reshape(kv_heads * group, rows),
    )


def pool_branch(pool_rows, pool_tail, mixing, scales, group_start, first_pos):
    rows = pool_rows.shape[0]
    columns = pool_rows.shape[1]
    pool_reach = max(POOL_SPANS)
    extended = jnp.concatenate([pool_tail, pool_rows], 0).astype(jnp.float32)
    group_index = group_start + jnp.arange(columns) // POOL_CH
    span_table = jnp.array(POOL_SPANS, jnp.int32)
    matches = group_index[:, None] == jnp.arange(len(POOL_SPANS))[None, :]
    span_of_col = jnp.sum(jnp.where(matches, span_table[None, :], 0), axis=1)
    trailing = jnp.zeros((rows, columns), jnp.float32)
    for lag in range(pool_reach):
        trailing = trailing + jnp.where(
            lag < span_of_col[None, :], extended[pool_reach - lag : pool_reach - lag + rows], 0.0
        )
    position = first_pos + jnp.arange(rows)
    count = jnp.minimum(position[:, None] + 1, span_of_col[None, :]).astype(jnp.float32)
    centred = (trailing / count - extended[pool_reach:]).astype(jnp.bfloat16)
    grouped = centred.reshape(rows, columns // POOL_CH, POOL_CH)
    product = jnp.einsum(
        "rgc,gcd->rgd", grouped, mixing, preferred_element_type=jnp.float32
    ).reshape(rows, columns)
    return (product * scales).astype(jnp.bfloat16)


def local(
    tokens,
    norm_gain,
    query_weight,
    key_matrix,
    value_matrix,
    pool_in_weight,
    head_sink_logit,
    pool_mix,
    pool_gain,
    attn_out_weight,
    pool_out_weight,
):
    tp_index = lax.axis_index("tp")
    sp_index = lax.axis_index("sp")
    q_cols = query_weight.shape[1]
    kv_cols = key_matrix.shape[1]
    pool_cols = pool_in_weight.shape[1]
    q_heads = q_cols // HEAD_SIZE
    kv_heads = kv_cols // HEAD_SIZE
    groups_dev = pool_cols // POOL_CH
    full_query, full_key, full_value, full_pool = (
        lax.all_gather(query_weight, "sp", axis=0, tiled=True),
        lax.all_gather(key_matrix, "sp", axis=0, tiled=True),
        lax.all_gather(value_matrix, "sp", axis=0, tiled=True),
        lax.all_gather(pool_in_weight, "sp", axis=0, tiled=True),
    )
    values_f = lax.all_gather(tokens[0], "tp", axis=0, tiled=True).astype(jnp.float32)
    scale = lax.rsqrt(jnp.mean(values_f * values_f, axis=-1, keepdims=True) + EPSILON)
    normed = (values_f * scale * norm_gain).astype(jnp.bfloat16)
    outputs = [
        jnp.dot(normed, weight, preferred_element_type=jnp.float32).astype(jnp.bfloat16)
        for weight in (full_query, full_key, full_value, full_pool)
    ]
    projected = jnp.concatenate(outputs, axis=1)
    rows = projected.shape[0]
    first_pos = sp_index * rows
    query_rows = projected[:, :q_cols]
    key_rows = projected[:, q_cols : q_cols + kv_cols]
    value_rows = projected[:, q_cols + kv_cols : q_cols + 2 * kv_cols]
    pool_rows = projected[:, q_cols + 2 * kv_cols :]
    pool_reach = max(POOL_SPANS)
    sinks = lax.dynamic_slice_in_dim(head_sink_logit, tp_index * q_heads, q_heads, 0)
    mixing = lax.dynamic_slice_in_dim(pool_mix, tp_index * groups_dev, groups_dev, 0)
    scales = lax.dynamic_slice_in_dim(pool_gain, tp_index * pool_cols, pool_cols, 0)
    key_tail, value_tail, pool_tail = passed_along(
        (key_rows[rows - WINDOW :], value_rows[rows - WINDOW :], pool_rows[rows - pool_reach :]),
        "sp",
        1,
    )
    attn_part, log_part = windowed_attend(
        query_rows,
        key_rows,
        value_rows,
        key_tail,
        value_tail,
        sinks,
        kv_heads,
        q_heads // kv_heads,
        first_pos,
    )
    pool_part = pool_branch(pool_rows, pool_tail, mixing, scales, tp_index * groups_dev, first_pos)
    half_attn, half_pool = (
        lax.all_gather(attn_out_weight, "sp", axis=1, tiled=True),
        lax.all_gather(pool_out_weight, "sp", axis=1, tiled=True),
    )
    result = lax.psum_scatter(
        jnp.dot(attn_part, half_attn, preferred_element_type=jnp.float32)
        + jnp.dot(pool_part, half_pool, preferred_element_type=jnp.float32),
        "tp",
        scatter_dimension=0,
        tiled=True,
    ).astype(jnp.bfloat16)
    return (result[None], log_part[None])


LANES = 128
TILE = 16
X_LAG, Y_LAG, LEAD = 2,6,1
CUTS, FAR_LAG = 1,0
MESH_ID = pl.DeviceIdType.MESH


def nearest(n, step, me):
    tables = [sorted((j for j in range(n) if j != z), key=lambda j: (abs(j - z), j)) for z in range(n)]
    shard = jnp.int32(tables[0][step])
    for z in range(1, n):
        shard = jnp.where(me == z, tables[z][step], shard)
    return shard


def layer_kernel(
    n,
    sinks,
    tokens,
    gain,
    wq,
    wk,
    wv,
    wp,
    mix,
    pool_gain,
    wao,
    wpo,
    out,
    log_out,
    held,
    tok,
    normed,
    proj,
    kv,
    pool_ext,
    mixed,
    mix_own,
    mine,
    sent,
    got,
    z_send,
    x_send,
    y_send,
    z_recv,
    x_recv,
    y_recv,
    load_sem,
    tok_sem,
    halo_send,
    halo_recv,
    sum_send,
    sum_recv,
):
    me = lax.axis_index("sp")
    f = lax.axis_index("fs")
    c = lax.axis_index("tp")
    f32 = jnp.float32
    half = tokens.shape[0]
    rows = 2 * half
    depth = wq.shape[0]
    n_in = (wq.shape[1] + wk.shape[1] + wv.shape[1] + wp.shape[1]) // LANES
    out_tiles = wao.shape[1] // LANES
    n_blocks = n_in + 2 * out_tiles
    steps = n_blocks // 3 * CUTS
    sources = [wk, wv] + [wq.at[:, pl.ds(i * LANES, LANES)] for i in range(wq.shape[1] // LANES)]
    sources += [wp.at[:, pl.ds(i * LANES, LANES)] for i in range(wp.shape[1] // LANES)]
    for i in range(out_tiles):
        sources += [w.at[:, pl.ds(i * LANES, LANES)] for w in (wao, wpo)]
    z_part = lax.rem(f, 3)
    beside = f + 1 - 2 * lax.rem(f, 2)
    across = lax.rem(f + 2, 4)
    x_part = lax.rem(beside, 3)
    y_part = 3 - z_part - x_part
    relays = (f == 0) | (f == 3)
    y_out = jnp.where(relays, x_part, z_part)
    up, down = me + 1, me - 1
    has_up, has_down = me < n - 1, me > 0

    def load(i):
        return pltpu.make_async_copy(sources[i], held.at[me, i], load_sem.at[i])

    for i in range(n_blocks):
        load(i).start()
    own_rows = pl.ds(pl.multiple_of(c * half, half), half)
    tok_load = pltpu.make_async_copy(tokens, tok.at[own_rows], tok_sem.at[2])
    tok_load.start()
    groups = mix_own.shape[0]
    mix_load = pltpu.make_async_copy(mix.at[pl.ds(c * groups, groups)], mix_own, tok_sem.at[3])
    mix_load.start()

    barrier = pltpu.get_barrier_semaphore()
    pl.semaphore_signal(barrier, inc=1, device_id={"tp": 1 - c}, device_id_type=MESH_ID)
    pl.semaphore_signal(barrier, inc=1, device_id={"fs": beside}, device_id_type=MESH_ID)
    pl.semaphore_signal(barrier, inc=1, device_id={"fs": across}, device_id_type=MESH_ID)

    @pl.when(has_up)
    def _():
        pl.semaphore_signal(barrier, inc=1, device_id={"sp": up}, device_id_type=MESH_ID)

    @pl.when(has_down)
    def _():
        pl.semaphore_signal(barrier, inc=1, device_id={"sp": down}, device_id_type=MESH_ID)

    pl.semaphore_wait(barrier, 3 + has_up.astype(jnp.int32) + has_down.astype(jnp.int32))

    tok_send = pltpu.make_async_remote_copy(
        tokens, tok.at[own_rows], tok_sem.at[0], tok_sem.at[1],
        device_id={"tp": 1 - c}, device_id_type=MESH_ID,
    )
    tok_send.start()

    def hop(s, j, part, send, recv, to):
        size = depth // CUTS
        block = held.at[j, 3 * (s // CUTS) + part, pl.ds(s % CUTS * size, size)]
        return pltpu.make_async_remote_copy(
            block, block, send, recv.at[s, j], device_id=to, device_id_type=MESH_ID
        )

    def z_hop(s, j, way):
        to = jnp.where(way == 0, up, down)
        return hop(s, j, z_part, z_send.at[way, s, j], z_recv, {"sp": to})

    def x_hop(s, j):
        return hop(s, j, z_part, x_send.at[s, j], x_recv, {"fs": beside})

    def y_hop(s, j):
        return hop(s, j, y_out, y_send.at[s, j], y_recv, {"fs": across})

    def onward(j):
        return jnp.where(j < me, 0, 1), ((j < me) & has_up) | ((j > me) & has_down)

    def own_send(s, finish=False):
        @pl.when(has_up)
        def _():
            cp = z_hop(s, me, 0)
            cp.wait_send() if finish else cp.start()

        @pl.when(has_down)
        def _():
            cp = z_hop(s, me, 1)
            cp.wait_send() if finish else cp.start()

    slots = [(s, k) for s in range(steps) for k in range(n - 1)]
    slots.sort(key=lambda slot: (slot[0] + FAR_LAG * slot[1], slot))
    shard = [nearest(n, k, me) for k in range(n - 1)]

    def z_step(t):
        s, k = slots[t]
        j = shard[k]
        if k == 0 and s + LEAD < steps:

            @pl.when(has_up & has_down)
            def _():
                own_send(s + LEAD)

        z_hop(s, j, 0).wait_recv()
        way, more = onward(j)

        @pl.when(more)
        def _():
            z_hop(s, j, way).start()

        x_hop(s, j).start()

        @pl.when(jnp.logical_not(relays))
        def _():
            y_hop(s, j).start()


    def x_step(t):
        s, k = slots[t]
        hop(s, shard[k], x_part, x_send.at[s, shard[k]], x_recv, {"fs": beside}).wait_recv()

        @pl.when(relays)
        def _():
            y_hop(s, shard[k]).start()


    def y_step(t):
        s, k = slots[t]
        hop(s, shard[k], y_part, y_send.at[s, shard[k]], y_recv, {"fs": across}).wait_recv()

    for i in range(n_blocks):
        load(i).wait()
        if i % 3 == 2:
            for s in range(i // 3 * CUTS, (i // 3 + 1) * CUTS):
                if s < LEAD:
                    own_send(s)
                else:

                    @pl.when(jnp.logical_not(has_up & has_down))
                    def _():
                        own_send(s)


    def norm_rows(r, size):
        v = tok[pl.ds(r, size), :].astype(f32)
        scale = lax.rsqrt(jnp.mean(v * v, axis=-1, keepdims=True) + EPSILON)
        normed[pl.ds(r, size), :] = (v * scale * gain[...]).astype(jnp.bfloat16)

    def norm_all():
        tok_load.wait()
        tok_send.wait()
        mix_load.wait()
        chunk = 32

        @pl.loop(0, rows // chunk)
        def _(i):
            norm_rows(pl.multiple_of(i * chunk, chunk), chunk)

    def project(pair):
        acc = None
        for j in range(n):
            w = jnp.concatenate([held[j, 2 * pair], held[j, 2 * pair + 1]], axis=1)
            term = jnp.dot(normed[:, j * depth : (j + 1) * depth], w, preferred_element_type=f32)
            acc = term if acc is None else acc + term
        return acc.astype(jnp.bfloat16)

    def halo_kv():
        return pltpu.make_async_remote_copy(
            kv.at[pl.ds(rows, WINDOW)], kv.at[pl.ds(0, WINDOW)], halo_send.at[0], halo_recv.at[0],
            device_id={"sp": up}, device_id_type=MESH_ID,
        )

    def halo_pool(g):
        return pltpu.make_async_remote_copy(
            pool_ext.at[g, pl.ds(rows, TILE)], pool_ext.at[g, pl.ds(0, TILE)],
            halo_send.at[1 + g], halo_recv.at[1 + g],
            device_id={"sp": up}, device_id_type=MESH_ID,
        )

    def first_zero(store):
        @pl.when(me == 0)
        def _():
            store()

    def project_kv():
        kv[pl.ds(WINDOW, rows), :] = project(0)

        @pl.when(has_up)
        def _():
            halo_kv().start()

        def zero():
            kv[pl.ds(0, WINDOW), :] = jnp.zeros((WINDOW, kv.shape[1]), kv.dtype)

        first_zero(zero)

    def project_q(g):
        proj[g] = project(1 + g)

    kv_cols = wk.shape[1]
    kv_heads = kv_cols // HEAD_SIZE
    group = wq.shape[1] // HEAD_SIZE // kv_heads

    def project_pool(g):
        pool_ext[g, pl.ds(TILE, rows), :] = project(1 + kv_heads + g)

        @pl.when(has_up)
        def _():
            halo_pool(g).start()

        def zero():
            pool_ext[g, pl.ds(0, TILE), :] = jnp.zeros((TILE, POOL_CH), pool_ext.dtype)

        first_zero(zero)

    def kv_arrived():
        @pl.when(has_down)
        def _():
            halo_kv().wait_recv()

    def attend(b):
        base = b * WINDOW
        lane = lax.broadcasted_iota(jnp.int32, (WINDOW, LANES), 1)
        logs = jnp.zeros((WINDOW, LANES), f32)
        i_pos = lax.broadcasted_iota(jnp.int32, (WINDOW, 2 * WINDOW), 0)
        k_pos = lax.broadcasted_iota(jnp.int32, (WINDOW, 2 * WINDOW), 1)
        allowed = (k_pos > i_pos) & (k_pos <= i_pos + WINDOW)
        allowed = allowed & (k_pos + (me * rows + base - WINDOW) >= 0)
        for g in range(kv_heads):
            band = kv[pl.ds(base, 2 * WINDOW), :]
            keys = band[:, g * HEAD_SIZE : (g + 1) * HEAD_SIZE]
            vals = band[:, kv_cols + g * HEAD_SIZE : kv_cols + (g + 1) * HEAD_SIZE]
            q = proj[g, pl.ds(base, WINDOW), :]
            q = jnp.concatenate([q[:, h * HEAD_SIZE : (h + 1) * HEAD_SIZE] for h in range(group)], axis=0)
            scores = lax.dot_general(q, keys, (((1,), (1,)), ((), ())), preferred_element_type=f32)
            probs = []
            for h in range(group):
                head = g * group + h
                sink = sinks[c * kv_heads * group + head]
                sc = jnp.where(allowed, scores[h * WINDOW : (h + 1) * WINDOW] * HEAD_SIZE**-0.5, -jnp.inf)
                top = jnp.maximum(jnp.max(sc, axis=-1, keepdims=True), sink)
                w = jnp.exp(sc - top)
                total = jnp.sum(w, axis=-1, keepdims=True) + jnp.exp(sink - top)
                probs.append((w * (1.0 / total)).astype(jnp.bfloat16))
                logs = jnp.where(lane == head, top + jnp.log(total), logs)
            res = jnp.dot(jnp.concatenate(probs, axis=0), vals, preferred_element_type=f32)
            res = jnp.concatenate([res[h * WINDOW : (h + 1) * WINDOW] for h in range(group)], axis=1)
            mixed[g, pl.ds(base, WINDOW), :] = res.astype(jnp.bfloat16)
        log_out[:, pl.ds(base, WINDOW)] = jnp.transpose(logs)[: kv_heads * group]

    def pool(g):
        @pl.when(has_down)
        def _():
            halo_pool(g).wait_recv()

        index = c * groups + g
        run = pool_ext[g].astype(f32)
        own = run[TILE:]
        trailing = jnp.zeros_like(run)
        span_here = jnp.int32(0)
        reach = 1
        for at, span in enumerate(POOL_SPANS):
            while reach < span:
                run = run + pltpu.roll(run, reach, 0)
                reach *= 2
            trailing = jnp.where(index == at, run, trailing)
            span_here = jnp.where(index == at, span, span_here)
        pos = me * rows + lax.broadcasted_iota(jnp.int32, (rows, 1), 0)
        count = jnp.minimum(pos + 1, span_here).astype(f32)
        centred = (trailing[TILE:] / count - own).astype(jnp.bfloat16)
        product = jnp.dot(centred, mix_own[g], preferred_element_type=f32)
        mixed[kv_heads + g] = (product * pool_gain[index]).astype(jnp.bfloat16)

    n_pairs = out_tiles // 2

    def sum_hop(slot):
        return pltpu.make_async_remote_copy(
            sent.at[slot], got.at[slot], sum_send.at[slot], sum_recv.at[slot],
            device_id={"tp": 1 - c}, device_id_type=MESH_ID,
        )

    def out_project(j, pair):
        slot = j * n_pairs + pair
        acc = None
        for side in range(2):
            first = n_in + 4 * pair + side
            w = jnp.concatenate([held[j, first], held[j, first + 2]], axis=1)
            parts = mixed.shape[0] // 2
            a = jnp.concatenate([mixed[side * parts + i] for i in range(parts)], axis=1)
            term = jnp.dot(a, w, preferred_element_type=f32)
            acc = term if acc is None else acc + term
        low, high = acc[:half], acc[half:]
        mine[slot] = jnp.where(c == 0, low, high)
        sent[slot] = jnp.where(c == 0, high, low)
        sum_hop(slot).start()

    def finish(j, pair):
        slot = j * n_pairs + pair
        sum_hop(slot).wait()
        wide = 2 * LANES
        cols = pl.ds(pl.multiple_of(slot * wide, wide), wide)
        out[:, cols] = (mine[slot] + got[slot]).astype(jnp.bfloat16)

    tasks = {}

    def ready(block):
        return slots.index((block // 3 * CUTS + CUTS - 1, n - 2))

    def at(t, task, *args):
        tasks.setdefault(min(t, len(slots) - 1), []).append((task, args))

    at(-1, norm_all)
    at(ready(1), project_kv)
    for g in range(kv_heads):
        at(ready(2 * g + 3), project_q, g)
    last = ready(2 * kv_heads + 1) + 1
    at(last, kv_arrived)
    for b in range(rows // WINDOW):
        at(last + b // 2, attend, b)
    for g in range(groups):
        at(ready(2 * (1 + kv_heads + g) + 1), project_pool, g)
    for g in range(groups):
        at(ready(2 * (kv_heads + groups) + 1) + (g + 1) // 2, pool, g)
    base_slot = ready(n_in - 1) + 1
    order = []
    for pair in range(n_pairs):
        at(base_slot, out_project, me, pair)
        order.append((base_slot, me, pair))
    for k in range(n - 1):
        for pair in range(n_pairs):
            when = slots.index(((n_in + 4 * pair + 3) // 3 * CUTS + CUTS - 1, k))
            at(max(when, base_slot), out_project, shard[k], pair)
            order.append((max(when, base_slot), shard[k], pair))

    late = []
    for when, j, pair in order:
        if when + 2 < len(slots) - 1:
            at(when + 2, finish, j, pair)
        else:
            late.append((j, pair))
    total_slots = len(slots)
    for t in range(total_slots + Y_LAG):
        if t < total_slots:
            z_step(t)
        if t == X_LAG - 1:
            for task, args in tasks.pop(-1, ()):
                task(*args)
        if 0 <= t - X_LAG < total_slots:
            x_step(t - X_LAG)
        if t >= Y_LAG:
            y_step(t - Y_LAG)
            for task, args in tasks.pop(t - Y_LAG, ()):
                task(*args)
    for j, pair in late:
        finish(j, pair)

    for s in range(steps):
        own_send(s, finish=True)
    for s, k in slots:
        way, more = onward(shard[k])

        @pl.when(more)
        def _():
            z_hop(s, shard[k], way).wait_send()

        x_hop(s, shard[k]).wait_send()
        y_hop(s, shard[k]).wait_send()

    @pl.when(has_up)
    def _():
        halo_kv().wait_send()
        for g in range(groups):
            halo_pool(g).wait_send()


def fused_local(
    n,
    tokens,
    norm_gain,
    query_weight,
    key_matrix,
    value_matrix,
    pool_in_weight,
    head_sink_logit,
    pool_mix,
    pool_gain,
    attn_out_weight,
    pool_out_weight,
):
    _, half, width = tokens.shape
    rows = 2 * half
    depth, q_cols = query_weight.shape
    kv_cols = key_matrix.shape[1]
    pool_cols = pool_in_weight.shape[1]
    heads = q_cols // HEAD_SIZE
    kv_heads = kv_cols // HEAD_SIZE
    groups = pool_cols // POOL_CH
    n_in = (q_cols + 2 * kv_cols + pool_cols) // LANES
    n_blocks = n_in + 2 * attn_out_weight.shape[1] // LANES
    steps = n_blocks // 3 * CUTS
    pieces = n * attn_out_weight.shape[1] // (2 * LANES)
    bf16, f32 = jnp.bfloat16, jnp.float32
    dma = pltpu.SemaphoreType.DMA
    hbm = pl.BlockSpec(memory_space=pl.ANY)
    vmem = pl.BlockSpec(memory_space=pltpu.VMEM)
    smem = pl.BlockSpec(memory_space=pltpu.SMEM)
    mixed, logs = pl.pallas_call(
        functools.partial(layer_kernel, n),
        out_shape=(
            jax.ShapeDtypeStruct((half, width), bf16),
            jax.ShapeDtypeStruct((heads, rows), f32),
        ),
        in_specs=[smem, hbm, vmem, hbm, hbm, hbm, hbm, hbm, vmem, hbm, hbm],
        out_specs=(vmem, vmem),
        scratch_shapes=[
            pltpu.VMEM((n, n_blocks, depth, LANES), bf16),
            pltpu.VMEM((rows, width), bf16),
            pltpu.VMEM((rows, width), bf16),
            pltpu.VMEM((kv_heads, rows, 2 * LANES), bf16),
            pltpu.VMEM((WINDOW + rows, 2 * kv_cols), bf16),
            pltpu.VMEM((groups, TILE + rows, POOL_CH), bf16),
            pltpu.VMEM((kv_heads + groups, rows, 2 * LANES), bf16),
            pltpu.VMEM((groups, POOL_CH, POOL_CH), bf16),
            pltpu.VMEM((pieces, half, 2 * LANES), f32),
            pltpu.VMEM((pieces, half, 2 * LANES), f32),
            pltpu.VMEM((pieces, half, 2 * LANES), f32),
            dma((2, steps, n)),
            dma((steps, n)),
            dma((steps, n)),
            dma((steps, n)),
            dma((steps, n)),
            dma((steps, n)),
            dma((n_blocks,)),
            dma((4,)),
            dma((1 + groups,)),
            dma((1 + groups,)),
            dma((pieces,)),
            dma((pieces,)),
        ],
        compiler_params=pltpu.CompilerParams(
            collective_id=0, has_side_effects=True, vmem_limit_bytes=60 * 1024 * 1024
        ),
    )(
        head_sink_logit,
        tokens[0],
        norm_gain.reshape(1, width),
        query_weight,
        key_matrix,
        value_matrix,
        pool_in_weight,
        pool_mix,
        pool_gain.reshape(-1, 1, POOL_CH),
        attn_out_weight,
        pool_out_weight,
    )
    return mixed[None], logs[None]


def fits(mesh, tokens, query_weight, key_matrix, pool_in_weight, attn_out_weight):
    n, f, c = mesh.shape["sp"], mesh.shape["fs"], mesh.shape["tp"]
    depth = query_weight.shape[0] // n
    rows = tokens.shape[1] // n
    q_cols, kv_cols, pool_cols = (w.shape[1] // c for w in (query_weight, key_matrix, pool_in_weight))
    tiles = attn_out_weight.shape[1] // n // LANES
    blocks = (q_cols + 2 * kv_cols + pool_cols) // LANES + 2 * tiles
    return (
        2 <= n <= 4
        and f == 4
        and c == 2
        and tokens.shape[0] == f
        and rows % WINDOW == 0
        and kv_cols == LANES
        and q_cols == 2 * LANES * (kv_cols // HEAD_SIZE)
        and pool_cols == q_cols
        and POOL_CH == 2 * LANES
        and attn_out_weight.shape[1] % (n * 2 * LANES) == 0
        and attn_out_weight.shape[0] // c == depth
        and depth % LANES == 0
        and blocks % 3 == 0
    )


def solution(mesh):
    in_specs = (
        P("fs", ("sp", "tp"), None),
        P(),
        P("sp", "tp"),
        P("sp", "tp"),
        P("sp", "tp"),
        P("sp", "tp"),
        P(),
        P(),
        P(),
        P("tp", "sp"),
        P("tp", "sp"),
    )
    out_specs = (P("fs", ("sp", "tp"), None), P("fs", "tp", "sp"))

    def step(*args):
        fused = fits(mesh, args[0], args[2], args[3], args[5], args[9])
        body = functools.partial(fused_local, mesh.shape["sp"]) if fused else local
        mapped = jax.shard_map(body, mesh=mesh, in_specs=in_specs, out_specs=out_specs, check_vma=False)
        return mapped(*args)

    return step
```

profile of v0, /device:TPU:0, one launch (start us, length us, event | category | flops | bytes accessed | tf_op | source)
XLA Modules:
  0.0 77.9 jit_solution(1119003590243579174)
XLA Ops:
  0.6 74.3 %shard_map.122 = (bf16[256,2048]{1,0:T(8,128)(2,1)}, f32[8,512]{1,0:T(8,128)}) custom-call(f32[16]{0:T(128)} %sinks.1, bf16[256,2048]{1,0:T(8,128)(2,1)} %bitcast.5, f32[1,2048]{1,0:T(1,128)} %bitcast.8, bf16[512,512]{1,0:T(8,128)(2,1)} %wq.1, bf16[512,128]{1,0:T(8,128)(2,1)} %wk.1, bf16[512,128]{1,0:T(8,128)(2,1)} %wv.1, bf16[512,512]{1,0:T(8,128)(2,1)} %wp.1, ...), custom_call_target="tpu_custom_call" | custom-call | tf_op jit(solution)/shard_map/pallas_call | solution.py:633
  75.0 0.0 copy-start
  75.0 2.3 %copy.15 = bf16[1,256,2048]{2,1,0:T(8,128)(2,1)} copy(bf16[1,256,2048]{2,1,0:T(8,128)(2,1)} %bitcast.6) | data formatting | bytes 2097152
  77.3 0.0 copy-done
  77.3 0.6 copy.16
Async XLA Ops:
  75.0 2.3 %copy-start = (f32[8,512]{1,0:T(8,128)S(1)}, f32[8,512]{1,0:T(8,128)}, u32[]{:S(2)}) copy-start(f32[8,512]{1,0:T(8,128)} %get-tuple-element.5) | copy-start | bytes 49156
where the time goes:
time: 79.4 us; the launch traced here: 77.9 us
  Pallas kernels  74.3 us (94%)
  local copies, waits for them, and re-layouts  2.92 us (4%)
    pallas_call x1, Pallas kernels, fused_local(): pl.pallas_call(functools.partial(layer_kernel, n), out_shape=(jax.ShapeDt...  74.3 us
    unnamed x4, local copies, waits for them, and re-layouts  2.92 us

commit v1 on v0

v1 whole, which is shorter than its diff:
```python
import functools

import jax
import jax.numpy as jnp
from jax import lax
from jax.experimental import pallas as pl
from jax.experimental.pallas import tpu as pltpu
from jax.sharding import PartitionSpec as P

HEAD_SIZE = 64
WINDOW = 128
POOL_CH = 256


EPSILON = 1e-06
POOL_SPANS = (2, 4, 8, 16)


def passed_along(shard, axis, by):
    size = lax.axis_size(axis)
    pairs = [(i, i + by) for i in range(size) if 0 <= i + by < size]
    return lax.ppermute(shard, axis, pairs)


def windowed_attend(
    query_rows, key_rows, value_rows, key_tail, value_tail, sinks, kv_heads, group, first_pos
):
    rows = query_rows.shape[0]
    blocks = rows // WINDOW
    width = key_rows.shape[1]
    ext_keys = jnp.concatenate([key_tail, key_rows], 0)
    ext_values = jnp.concatenate([value_tail, value_rows], 0)

    def banded(table):
        return jnp.concatenate(
            [
                table[:rows].reshape(blocks, WINDOW, width),
                table[WINDOW:].reshape(blocks, WINDOW, width),
            ],
            axis=1,
        )

    band_keys = banded(ext_keys).reshape(blocks, 2 * WINDOW, kv_heads, HEAD_SIZE)
    band_values = banded(ext_values).reshape(blocks, 2 * WINDOW, kv_heads, HEAD_SIZE)
    query_blocks = query_rows.reshape(blocks, WINDOW, kv_heads, group, HEAD_SIZE)
    scores = jnp.einsum(
        "bqkgd,bskd->bkgqs", query_blocks, band_keys, preferred_element_type=jnp.float32
    ) * HEAD_SIZE ** (-0.5)
    query_pos = first_pos + jnp.arange(rows).reshape(blocks, WINDOW, 1)
    key_pos = (
        first_pos
        - WINDOW
        + jnp.arange(blocks).reshape(blocks, 1, 1) * WINDOW
        + jnp.arange(2 * WINDOW).reshape(1, 1, 2 * WINDOW)
    )
    offset = query_pos - key_pos
    allowed = (offset >= 0) & (offset < WINDOW) & (key_pos >= 0)
    scores = jnp.where(allowed[:, None, None], scores, -jnp.inf)
    sink_grid = sinks.reshape(1, kv_heads, group, 1, 1)
    top = jnp.maximum(jnp.max(scores, axis=-1, keepdims=True), sink_grid)
    weights = jnp.exp(scores - top)
    total = jnp.sum(weights, axis=-1, keepdims=True) + jnp.exp(sink_grid - top)
    probs = (weights / total).astype(jnp.bfloat16)
    mixed = jnp.einsum(
        "bkgqs,bskd->bqkgd", probs, band_values, preferred_element_type=jnp.float32
    ).astype(jnp.bfloat16)
    row_log_weight_sum = (top + jnp.log(total))[..., 0]
    return (
        mixed.reshape(rows, kv_heads * group * HEAD_SIZE),
        row_log_weight_sum.transpose(1, 2, 0, 3).reshape(kv_heads * group, rows),
    )


def pool_branch(pool_rows, pool_tail, mixing, scales, group_start, first_pos):
    rows = pool_rows.shape[0]
    columns = pool_rows.shape[1]
    pool_reach = max(POOL_SPANS)
    extended = jnp.concatenate([pool_tail, pool_rows], 0).astype(jnp.float32)
    group_index = group_start + jnp.arange(columns) // POOL_CH
    span_table = jnp.array(POOL_SPANS, jnp.int32)
    matches = group_index[:, None] == jnp.arange(len(POOL_SPANS))[None, :]
    span_of_col = jnp.sum(jnp.where(matches, span_table[None, :], 0), axis=1)
    trailing = jnp.zeros((rows, columns), jnp.float32)
    for lag in range(pool_reach):
        trailing = trailing + jnp.where(
            lag < span_of_col[None, :], extended[pool_reach - lag : pool_reach - lag + rows], 0.0
        )
    position = first_pos + jnp.arange(rows)
    count = jnp.minimum(position[:, None] + 1, span_of_col[None, :]).astype(jnp.float32)
    centred = (trailing / count - extended[pool_reach:]).astype(jnp.bfloat16)
    grouped = centred.reshape(rows, columns // POOL_CH, POOL_CH)
    product = jnp.einsum(
        "rgc,gcd->rgd", grouped, mixing, preferred_element_type=jnp.float32
    ).reshape(rows, columns)
    return (product * scales).astype(jnp.bfloat16)


def local(
    tokens,
    norm_gain,
    query_weight,
    key_matrix,
    value_matrix,
    pool_in_weight,
    head_sink_logit,
    pool_mix,
    pool_gain,
    attn_out_weight,
    pool_out_weight,
):
    tp_index = lax.axis_index("tp")
    sp_index = lax.axis_index("sp")
    q_cols = query_weight.shape[1]
    kv_cols = key_matrix.shape[1]
    pool_cols = pool_in_weight.shape[1]
    q_heads = q_cols // HEAD_SIZE
    kv_heads = kv_cols // HEAD_SIZE
    groups_dev = pool_cols // POOL_CH
    full_query, full_key, full_value, full_pool = (
        lax.all_gather(query_weight, "sp", axis=0, tiled=True),
        lax.all_gather(key_matrix, "sp", axis=0, tiled=True),
        lax.all_gather(value_matrix, "sp", axis=0, tiled=True),
        lax.all_gather(pool_in_weight, "sp", axis=0, tiled=True),
    )
    values_f = lax.all_gather(tokens[0], "tp", axis=0, tiled=True).astype(jnp.float32)
    scale = lax.rsqrt(jnp.mean(values_f * values_f, axis=-1, keepdims=True) + EPSILON)
    normed = (values_f * scale * norm_gain).astype(jnp.bfloat16)
    outputs = [
        jnp.dot(normed, weight, preferred_element_type=jnp.float32).astype(jnp.bfloat16)
        for weight in (full_query, full_key, full_value, full_pool)
    ]
    projected = jnp.concatenate(outputs, axis=1)
    rows = projected.shape[0]
    first_pos = sp_index * rows
    query_rows = projected[:, :q_cols]
    key_rows = projected[:, q_cols : q_cols + kv_cols]
    value_rows = projected[:, q_cols + kv_cols : q_cols + 2 * kv_cols]
    pool_rows = projected[:, q_cols + 2 * kv_cols :]
    pool_reach = max(POOL_SPANS)
    sinks = lax.dynamic_slice_in_dim(head_sink_logit, tp_index * q_heads, q_heads, 0)
    mixing = lax.dynamic_slice_in_dim(pool_mix, tp_index * groups_dev, groups_dev, 0)
    scales = lax.dynamic_slice_in_dim(pool_gain, tp_index * pool_cols, pool_cols, 0)
    key_tail, value_tail, pool_tail = passed_along(
        (key_rows[rows - WINDOW :], value_rows[rows - WINDOW :], pool_rows[rows - pool_reach :]),
        "sp",
        1,
    )
    attn_part, log_part = windowed_attend(
        query_rows,
        key_rows,
        value_rows,
        key_tail,
        value_tail,
        sinks,
        kv_heads,
        q_heads // kv_heads,
        first_pos,
    )
    pool_part = pool_branch(pool_rows, pool_tail, mixing, scales, tp_index * groups_dev, first_pos)
    half_attn, half_pool = (
        lax.all_gather(attn_out_weight, "sp", axis=1, tiled=True),
        lax.all_gather(pool_out_weight, "sp", axis=1, tiled=True),
    )
    result = lax.psum_scatter(
        jnp.dot(attn_part, half_attn, preferred_element_type=jnp.float32)
        + jnp.dot(pool_part, half_pool, preferred_element_type=jnp.float32),
        "tp",
        scatter_dimension=0,
        tiled=True,
    ).astype(jnp.bfloat16)
    return (result[None], log_part[None])


LANES = 128
TILE = 16
OUT_CUTS = 4
MESH_ID = pl.DeviceIdType.MESH


def nearest(n, step, me):
    tables = [sorted((j for j in range(n) if j != z), key=lambda j: (abs(j - z), j)) for z in range(n)]
    shard = jnp.int32(tables[0][step])
    for z in range(1, n):
        shard = jnp.where(me == z, tables[z][step], shard)
    return shard


def layer_kernel(
    n,
    sinks,
    tokens,
    gain,
    wq,
    wk,
    wv,
    wp,
    mix,
    pool_gain,
    wao,
    wpo,
    out,
    log_out,
    held,
    wout,
    kv_in,
    tok,
    gain_v,
    pgain_v,
    sink_v,
    out_v,
    log_v,
    acc_q,
    acc_p,
    nrm,
    qb,
    kvb,
    pool_ext,
    mixed,
    mix_own,
    logs,
    logs_got,
    keep_n,
    send_n,
    got_n,
    y_part,
    y_got,
    mine,
    sent,
    got,
    z_send,
    x_send,
    z_recv,
    x_recv,
    load_sem,
    tok_sem,
    tok_send,
    tok_recv,
    ytok_send,
    ytok_recv,
    fwd_send,
    fwd_recv,
    halo_send,
    halo_recv,
    sumn_send,
    sumn_recv,
    sumo_send,
    sumo_recv,
    yp_send,
    yp_recv,
    log_send,
    log_recv,
    out_sem,
):
    me = lax.axis_index("sp")
    f = lax.axis_index("fs")
    c = lax.axis_index("tp")
    f32, bf16 = jnp.float32, jnp.bfloat16
    half, width = tokens.shape
    rows = 2 * half
    depth = wq.shape[0]
    part_rows = depth // 2
    q_cols = wq.shape[1] // 2
    group = q_cols // HEAD_SIZE
    out_cols = wao.shape[1]
    n_in = held.shape[1]
    n_pieces = n_in + OUT_CUTS
    chunk = half // 4
    blocks = rows // WINDOW
    y, x = f // 2, lax.rem(f, 2)
    beside = f + 1 - 2 * x
    across = lax.rem(f + 2, 4)
    up, down = me + 1, me - 1
    has_up, has_down = me < n - 1, me > 0
    inner = has_up & has_down

    def at_cols(ref, i):
        return ref.at[:, pl.ds(pl.multiple_of(y * q_cols + i * LANES, LANES), LANES)]

    y_rows = pl.ds(pl.multiple_of(y * part_rows, part_rows), part_rows)
    pool_index = 2 * c + y
    norm_order = (2, 0, 1, 3)

    def own_chunk(i, side):
        first = (3, 1, 2, 0) if side == 0 else (0, 2, 1, 3)
        return first[i] * chunk

    def own_at(i):
        return pl.multiple_of(jnp.where(c == 0, own_chunk(i, 0), own_chunk(i, 1)), chunk)

    def tok_load(i):
        at = pl.ds(own_at(i), chunk)
        return pltpu.make_async_copy(tokens.at[at], tok.at[at], tok_sem.at[i])

    first_loads = [
        pltpu.make_async_copy(wk, kv_in.at[0], load_sem.at[0]),
        pltpu.make_async_copy(wv, kv_in.at[1], load_sem.at[0]),
    ]
    for i in range(2):
        first_loads.append(pltpu.make_async_copy(at_cols(wq, i), held.at[me, 1 + i], load_sem.at[0]))
    for i in range(2):
        first_loads.append(pltpu.make_async_copy(at_cols(wp, i), held.at[me, 3 + i], load_sem.at[0]))
    late_loads = [
        pltpu.make_async_copy(wao.at[y_rows], wout.at[me, pl.ds(0, part_rows)], load_sem.at[1]),
        pltpu.make_async_copy(wpo.at[y_rows], wout.at[me, pl.ds(part_rows, part_rows)], load_sem.at[2]),
        pltpu.make_async_copy(mix.at[pool_index], mix_own, load_sem.at[3]),
        pltpu.make_async_copy(pool_gain, pgain_v, load_sem.at[4]),
        pltpu.make_async_copy(sinks, sink_v, load_sem.at[5]),
    ]
    gain_load = pltpu.make_async_copy(gain, gain_v, load_sem.at[6])
    for cp in first_loads[:2]:
        cp.start()
    tok_load(norm_order[0]).start()
    gain_load.start()
    for cp in first_loads[2:]:
        cp.start()
    for i in norm_order[1:]:
        tok_load(i).start()
    for cp in late_loads:
        cp.start()

    barrier = pltpu.get_barrier_semaphore()
    for peer in ({"tp": 1 - c}, {"fs": beside}, {"fs": across}, {"fs": across, "tp": 1 - c}):
        pl.semaphore_signal(barrier, inc=1, device_id=peer, device_id_type=MESH_ID)

    @pl.when(has_up)
    def _():
        pl.semaphore_signal(barrier, inc=1, device_id={"sp": up}, device_id_type=MESH_ID)

    @pl.when(has_down)
    def _():
        pl.semaphore_signal(barrier, inc=1, device_id={"sp": down}, device_id_type=MESH_ID)

    def remote(src, dst, send, recv, to):
        return pltpu.make_async_remote_copy(src, dst, send, recv, device_id=to, device_id_type=MESH_ID)

    def piece(s, j, part):
        if s < n_in:
            return held.at[j, s, pl.ds(pl.multiple_of(part * part_rows, part_rows), part_rows)]
        size = part_rows // OUT_CUTS
        return wout.at[j, pl.ds(pl.multiple_of(part * part_rows + (s - n_in) * size, size), size)]

    def bulk(count):
        return nrm.at[0, pl.ds(0, count * part_rows * LANES // width)]

    def sent_all(ref, sem):
        pltpu.make_async_remote_copy(ref, ref, sem, sem, device_id={"tp": 1 - c}, device_id_type=MESH_ID).wait_send()

    def got_all(ref, sem):
        pltpu.make_async_remote_copy(ref, ref, sem, sem, device_id={"tp": 1 - c}, device_id_type=MESH_ID).wait_recv()

    def z_hop(s, j, way):
        block = piece(s, j, x)
        to = me if way is None else jnp.where(way == 0, up, down)
        slot = z_recv.at[s, lax.rem(j - to + n, n) - 1]
        return remote(block, block, z_send.at[0 if way is None else way], slot, {"sp": to})

    def x_group(s, k):
        if s >= n_in:
            return 5 + k
        return 0 if s == 0 else 1 + 2 * ((s - 1) // 2) + k // (n - 2)

    def x_hop(s, k):
        block = piece(s, shard[k], x)
        return remote(block, block, x_send, x_recv.at[x_group(s, k)], {"fs": beside})

    def onward(j):
        return jnp.where(j < me, 0, 1), ((j < me) & has_up) | ((j > me) & has_down)

    def own_send(s):
        @pl.when(has_up)
        def _():
            z_hop(s, me, 0).start()

        @pl.when(has_down)
        def _():
            z_hop(s, me, 1).start()

    shard = [nearest(n, k, me) for k in range(n - 1)]
    def pass_on(s, k):
        j = shard[k]
        z_hop(s, j, None).wait_recv()
        way, more = onward(j)

        @pl.when(more)
        def _():
            z_hop(s, j, way).start()

        x_hop(s, k).start()

    def inner_slot(s, k):
        @pl.when(inner)
        def _():
            pass_on(s, k)

    def end_slot(s, k):
        @pl.when(jnp.logical_not(inner))
        def _():
            pass_on(s, k)

    def send_inner(s):
        @pl.when(inner)
        def _():
            own_send(s)

    def send_end(s):
        @pl.when(jnp.logical_not(inner))
        def _():
            own_send(s)

    def pick(a, b):
        return pl.ds(pl.multiple_of(jnp.where(c == 0, a, b), chunk), chunk)

    def tok_hop(i):
        block = nrm.at[0, pick(own_chunk(i, 0), half + own_chunk(i, 1))]
        return remote(block, block, tok_send, tok_recv, {"tp": 1 - c})

    low_order = (2, 4, 6, 0)
    high_order = (5, 3, 7, 1)

    def y_tok(i):
        where = pick(low_order[i] * chunk, high_order[i] * chunk)
        return remote(nrm.at[0, where], nrm.at[1, where], ytok_send, ytok_recv.at[i], {"fs": across})

    def fwd(i):
        block = nrm.at[1, pick(low_order[i] * chunk, high_order[i] * chunk)]
        return remote(block, block, fwd_send, fwd_recv.at[i], {"tp": 1 - c})

    @pl.when(me == 0)
    def _():
        for s in range(2):
            kvb[s, pl.ds(0, WINDOW), :] = jnp.zeros((WINDOW, kvb.shape[2]), bf16)
            pool_ext[s, pl.ds(0, TILE), :] = jnp.zeros((TILE, POOL_CH), bf16)

    first = nrm.at[0, pl.ds(0, len(first_loads) * depth * LANES // width)]
    pltpu.make_async_copy(first, first, load_sem.at[0]).wait()
    k_all, v_all = kv_in[0], kv_in[1]
    first = jnp.concatenate([k_all[:, :HEAD_SIZE], v_all[:, :HEAD_SIZE]], axis=1)
    second = jnp.concatenate([k_all[:, HEAD_SIZE:], v_all[:, HEAD_SIZE:]], axis=1)
    held[me, 0] = jnp.where(y == 0, first, second)
    gain_load.wait()
    pl.semaphore_wait(barrier, 4 + has_up.astype(jnp.int32) + has_down.astype(jnp.int32))
    strip = 32

    def norm(i):
        tok_load(i).wait()
        for part in range(chunk // strip):
            at = pl.multiple_of(own_at(i) + part * strip, strip)
            v = tok[pl.ds(at, strip), :].astype(f32)
            scale = lax.rsqrt(jnp.mean(v * v, axis=-1, keepdims=True) + EPSILON)
            nrm[0, pl.ds(pl.multiple_of(c * half + at, strip), strip), :] = (v * scale * gain_v[...]).astype(bf16)
        if i == norm_order[0]:
            y_tok(0).start()
        tok_hop(i).start()

    def own_tokens():
        got_all(nrm.at[0, pl.ds(0, half)], tok_recv)
        for i in range(1, 4):
            y_tok(i).start()

    def y_service(i):
        y_tok(i).wait_recv()
        fwd(i).start()

    def project(s, r0, size, cols, shards, acc=None):
        for j in shards:
            w = held[j, cols[0]] if len(cols) == 1 else jnp.concatenate([held[j, b] for b in cols], axis=1)
            deep = slice(j * depth, (j + 1) * depth) if isinstance(j, int) else pl.ds(pl.multiple_of(j * depth, depth), depth)
            term = jnp.dot(nrm[s, r0 : r0 + size, deep], w, preferred_element_type=f32)
            acc = term if acc is None else acc + term
        return acc

    every = range(n)
    early, last = [me] + shard[:-1], shard[-1:]

    def halo_kv(s):
        return remote(
            kvb.at[s, pl.ds(rows, WINDOW)], kvb.at[s, pl.ds(0, WINDOW)], halo_send.at[s], halo_recv.at[s], {"sp": up}
        )

    def halo_pool(s):
        return remote(
            pool_ext.at[s, pl.ds(rows, TILE)],
            pool_ext.at[s, pl.ds(0, TILE)],
            halo_send.at[2 + s],
            halo_recv.at[2 + s],
            {"sp": up},
        )

    def send_halo(halo, s):
        @pl.when(has_up)
        def _():
            halo(s).start()

    def wait_halo(halo, s):
        @pl.when(has_down)
        def _():
            halo(s).wait_recv()

    def project_kv(s, r0, size):
        kvb[s, pl.ds(WINDOW + r0, size), :] = project(s, r0, size, [0], every).astype(bf16)

    def project_q(s, r0, size):
        qb[s, pl.ds(r0, size), :] = project(s, r0, size, [1, 2], every).astype(bf16)

    def begin_q(s, r0, size):
        acc_q[s, pl.ds(r0, size), :] = project(s, r0, size, [1, 2], early)

    def end_q(s, r0, size):
        qb[s, pl.ds(r0, size), :] = project(s, r0, size, [1, 2], last, acc_q[s, pl.ds(r0, size), :]).astype(bf16)

    def project_pool(s, r0, size):
        pool_ext[s, pl.ds(TILE + r0, size), :] = project(s, r0, size, [3, 4], every).astype(bf16)

    def begin_pool(s, r0, size):
        acc_p[s, pl.ds(r0, size), :] = project(s, r0, size, [3, 4], early)

    def end_pool(s, r0, size):
        done = project(s, r0, size, [3, 4], last, acc_p[s, pl.ds(r0, size), :])
        pool_ext[s, pl.ds(TILE + r0, size), :] = done.astype(bf16)

    def attend(s, b):
        base = b * WINDOW
        lane = lax.broadcasted_iota(jnp.int32, (WINDOW, LANES), 1)
        lgs = jnp.zeros((WINDOW, LANES), f32)
        i_pos = lax.broadcasted_iota(jnp.int32, (WINDOW, 2 * WINDOW), 0)
        k_pos = lax.broadcasted_iota(jnp.int32, (WINDOW, 2 * WINDOW), 1)
        allowed = (k_pos > i_pos) & (k_pos <= i_pos + WINDOW)
        if b == 0:
            allowed = allowed & (k_pos + (me * rows - WINDOW) >= 0)
        band = kvb[s, pl.ds(base, 2 * WINDOW), :]
        keys, vals = band[:, :HEAD_SIZE], band[:, HEAD_SIZE:]
        q = qb[s, pl.ds(base, WINDOW), :]
        q = jnp.concatenate([q[:, h * HEAD_SIZE : (h + 1) * HEAD_SIZE] for h in range(group)], axis=0)
        scores = lax.dot_general(q, keys, (((1,), (1,)), ((), ())), preferred_element_type=f32)
        probs = []
        for h in range(group):
            sink = sink_v[(2 * c + y) * group + h]
            sc = jnp.where(allowed, scores[h * WINDOW : (h + 1) * WINDOW] * HEAD_SIZE**-0.5, -jnp.inf)
            top = jnp.maximum(jnp.max(sc, axis=-1, keepdims=True), sink)
            w = jnp.exp(sc - top)
            total = jnp.sum(w, axis=-1, keepdims=True) + jnp.exp(sink - top)
            probs.append((w * (1.0 / total)).astype(bf16))
            lgs = jnp.where(lane == h, top + jnp.log(total), lgs)
        res = jnp.dot(jnp.concatenate(probs, axis=0), vals, preferred_element_type=f32)
        res = jnp.concatenate([res[h * WINDOW : (h + 1) * WINDOW] for h in range(group)], axis=1)
        mixed[s, pl.ds(base, WINDOW), pl.ds(0, q_cols)] = res.astype(bf16)
        logs[s, :, pl.ds(base, WINDOW)] = jnp.transpose(lgs)[: logs.shape[1]]

    def pool(s, part):
        base = part * half
        run = pool_ext[s, pl.ds(base, TILE + half), :].astype(f32)
        own = run[TILE:]
        trailing = jnp.zeros_like(run)
        span_here = jnp.int32(0)
        reach = 1
        for at, span in enumerate(POOL_SPANS):
            while reach < span:
                run = run + pltpu.roll(run, reach, 0)
                reach *= 2
            trailing = jnp.where(pool_index == at, run, trailing)
            span_here = jnp.where(pool_index == at, span, span_here)
        pos = me * rows + base + lax.broadcasted_iota(jnp.int32, (half, 1), 0)
        count = jnp.minimum(pos + 1, span_here).astype(f32)
        centred = (trailing[TILE:] / count - own).astype(bf16)
        product = jnp.dot(centred, mix_own[...], preferred_element_type=f32)
        mixed[s, pl.ds(base, half), pl.ds(q_cols, POOL_CH)] = (product * pgain_v[pool_index]).astype(bf16)

    def log_hop():
        return remote(logs.at[1], logs_got, log_send, log_recv, {"fs": across})

    order = [me] + shard
    wide = out_cols // 2

    def sum_n(part, i):
        u = i * 2 + part
        return remote(send_n.at[u], got_n.at[u], sumn_send, sumn_recv.at[u], {"tp": 1 - c})

    def sum_o(i):
        return remote(sent.at[i], got.at[i], sumo_send, sumo_recv.at[i], {"tp": 1 - c})

    def y_sum(part, i):
        return remote(
            y_part.at[i * 2 + part], y_got.at[i, c], yp_send, yp_recv.at[i], {"fs": across, "tp": part}
        )

    def out_far(part, i):
        u = i * 2 + part
        acc = jnp.dot(mixed[1, part * half : (part + 1) * half, :], wout[order[i]], preferred_element_type=f32)
        left, right = acc[:, :wide], acc[:, wide:]
        keep_n[u] = jnp.where(c == 0, left, right)
        send_n[u] = jnp.where(c == 0, right, left)
        sum_n(part, i).start()

    def pass_far(part, i):
        u = i * 2 + part
        sum_n(part, i).wait_recv()
        y_part[u] = (keep_n[u] + got_n[u]).astype(bf16)
        y_sum(part, i).start()

    def out_own(i):
        acc = jnp.dot(mixed[0], wout[order[i]], preferred_element_type=f32)
        low, high = acc[:half], acc[half:]
        mine[i] = jnp.where(c == 0, low, high)
        sent[i] = jnp.where(c == 0, high, low)
        sum_o(i).start()

    def finish(i):
        sum_o(i).wait_recv()
        got_all(y_got.at[i], yp_recv.at[i])
        there = jnp.concatenate([y_got[i, 0], y_got[i, 1]], axis=1).astype(f32)
        out_v[i] = (mine[i] + got[i] + there).astype(bf16)
        out_copy(i).start()

    def out_copy(i):
        cols = pl.ds(pl.multiple_of(order[i] * out_cols, out_cols), out_cols)
        return pltpu.make_async_copy(out_v.at[i], out.at[:, cols], out_sem.at[0])

    log_copy = pltpu.make_async_copy(log_v, log_out, out_sem.at[1])

    def send_log():
        log_hop().start()

    def write_log():
        log_hop().wait()
        own_logs, far_logs = logs[0, :group], logs_got[:group]
        log_v[...] = jnp.where(
            y == 0, jnp.concatenate([own_logs, far_logs], axis=0), jnp.concatenate([far_logs, own_logs], axis=0)
        )
        log_copy.start()

    def drain():
        for z in range(n):

            @pl.when(me == z)
            def _():
                if z < n - 1:
                    sent_all(bulk(n_pieces * (z + 1)), z_send.at[0])
                if z:
                    sent_all(bulk(n_pieces * (n - z)), z_send.at[1])

        sent_all(bulk(n_pieces * (n - 1)), x_send)
        for sem in (tok_send, ytok_send, fwd_send):
            sent_all(nrm.at[0, pl.ds(0, half)], sem)

        @pl.when(has_up)
        def _():
            for s in range(2):
                halo_kv(s).wait_send()
                halo_pool(s).wait_send()

    def ready(pieces, ks):
        got_all(bulk(len(pieces) * len(ks)), x_recv.at[x_group(pieces[0], ks[0])])

    def ready_out(k):
        got_all(bulk(OUT_CUTS), x_recv.at[x_group(n_in, k)])

    def arrived(i):
        fwd(i).wait_recv()

    def late_wait():
        for cp in late_loads:
            cp.wait()

    W = WINDOW
    send_end(1)
    send_inner(1)
    norm(2)
    norm(0)
    norm(1)
    norm(3)
    send_end(2)
    send_inner(2)
    send_inner(0)
    send_end(0)
    inner_slot(1, 0)
    inner_slot(1, 1)
    send_end(3)
    inner_slot(2, 0)
    send_end(4)
    end_slot(1, 0)
    inner_slot(2, 1)
    end_slot(2, 0)
    own_tokens()
    end_slot(0, 0)
    end_slot(1, 1)
    end_slot(2, 1)
    inner_slot(0, 1)
    end_slot(0, 1)
    inner_slot(0, 0)
    end_slot(1, 2)
    inner_slot(1, 2)
    y_service(0)
    late_wait()
    send_end(8)
    end_slot(2, 2)
    inner_slot(2, 2)
    inner_slot(0, 2)
    send_inner(4)
    send_inner(3)
    y_service(1)
    ready([1, 2], range(n - 2))
    begin_q(0, half, half)
    end_slot(0, 2)
    send_end(6)
    arrived(0)
    inner_slot(4, 0)
    inner_slot(4, 1)
    inner_slot(3, 1)
    inner_slot(3, 0)
    end_slot(4, 0)
    begin_q(0, 0, half)
    ready([1, 2], [n - 2])
    end_q(0, 0, half)
    end_slot(3, 0)
    inner_slot(4, 2)
    arrived(1)
    begin_q(1, W, 2 * W)
    ready([0], range(n - 1))
    project_kv(0, 0, half)
    end_q(0, half, half)
    end_slot(4, 1)
    send_end(5)
    inner_slot(3, 2)
    send_inner(5)
    project_kv(0, half, half)
    attend(0, 2)
    y_service(2)
    end_slot(3, 1)
    send_inner(6)
    send_end(7)
    send_inner(8)
    attend(0, 1)
    project_kv(1, W, 2 * W)
    end_slot(4, 2)
    attend(0, 3)
    arrived(2)
    project_kv(1, 3 * W, W)
    send_halo(halo_kv, 1)
    send_inner(7)
    inner_slot(5, 1)
    inner_slot(5, 0)
    end_slot(3, 2)
    end_q(1, W, 2 * W)
    attend(1, 2)
    ready([3, 4], range(n - 2))
    begin_pool(0, half, half)
    end_slot(5, 0)
    y_service(3)
    begin_q(1, 3 * W, W)
    end_q(1, 3 * W, W)
    attend(1, 3)
    end_slot(6, 0)
    begin_pool(1, half - TILE, half + TILE)
    ready([3, 4], [n - 2])
    end_pool(1, half - TILE, half + TILE)
    send_halo(halo_pool, 1)
    inner_slot(6, 0)
    pool(1, 1)
    out_far(1, 0)
    end_pool(0, half, half)
    send_halo(halo_pool, 0)
    inner_slot(7, 0)
    send_halo(halo_kv, 0)
    inner_slot(8, 0)
    inner_slot(6, 1)
    end_slot(8, 0)
    inner_slot(7, 1)
    inner_slot(8, 1)
    arrived(3)
    project_kv(1, 0, W)
    attend(1, 1)
    wait_halo(halo_kv, 1)
    project_q(1, 0, W)
    attend(1, 0)
    send_log()
    pass_far(1, 0)
    inner_slot(5, 2)
    end_slot(7, 0)
    project_pool(1, 0, half - TILE)
    wait_halo(halo_pool, 1)
    pool(1, 0)
    out_far(0, 0)
    end_slot(5, 1)
    begin_pool(0, 0, half)
    end_pool(0, 0, half)
    pool(0, 1)
    wait_halo(halo_pool, 0)
    pool(0, 0)
    inner_slot(7, 2)
    end_slot(6, 1)
    inner_slot(6, 2)
    ready_out(0)
    out_far(0, 1)
    inner_slot(8, 2)
    end_slot(7, 1)
    pass_far(0, 0)
    out_far(1, 1)
    wait_halo(halo_kv, 0)
    attend(0, 0)
    out_own(0)
    end_slot(8, 1)
    out_own(1)
    pass_far(0, 1)
    pass_far(1, 1)
    end_slot(5, 2)
    end_slot(7, 2)
    finish(0)
    ready_out(1)
    out_far(1, 2)
    out_far(0, 2)
    end_slot(6, 2)
    out_own(2)
    end_slot(8, 2)
    drain()
    write_log()
    pass_far(1, 2)
    pass_far(0, 2)
    finish(1)
    ready_out(2)
    out_far(0, 3)
    out_far(1, 3)
    out_own(3)
    pass_far(0, 3)
    pass_far(1, 3)
    finish(2)
    finish(3)
    sent_all(send_n, sumn_send)
    sent_all(sent, sumo_send)
    sent_all(y_part, yp_send)
    pltpu.make_async_copy(out, out, out_sem.at[0]).wait()
    log_copy.wait()


def fused_local(
    n,
    tokens,
    norm_gain,
    query_weight,
    key_matrix,
    value_matrix,
    pool_in_weight,
    head_sink_logit,
    pool_mix,
    pool_gain,
    attn_out_weight,
    pool_out_weight,
):
    _, half, width = tokens.shape
    rows = 2 * half
    depth, q_all = query_weight.shape
    heads = q_all // HEAD_SIZE
    kv_cols = key_matrix.shape[1]
    q_cols = q_all // 2
    out_cols = attn_out_weight.shape[1]
    n_in = 1 + 2 * (q_cols // LANES)
    pieces = n_in + OUT_CUTS
    bf16, f32 = jnp.bfloat16, jnp.float32
    dma = pltpu.SemaphoreType.DMA
    hbm = pl.BlockSpec(memory_space=pl.ANY)
    mixed, logs = pl.pallas_call(
        functools.partial(layer_kernel, n),
        out_shape=(
            jax.ShapeDtypeStruct((half, width), bf16),
            jax.ShapeDtypeStruct((heads, rows), f32),
        ),
        in_specs=[hbm] * 11,
        out_specs=(hbm, hbm),
        scratch_shapes=[
            pltpu.VMEM((n, n_in, depth, LANES), bf16),
            pltpu.VMEM((n, depth, out_cols), bf16),
            pltpu.VMEM((2, depth, kv_cols), bf16),
            pltpu.VMEM((half, width), bf16),
            pltpu.VMEM((1, width), f32),
            pltpu.VMEM((2 * 2, 1, POOL_CH), f32),
            pltpu.SMEM(head_sink_logit.shape, f32),
            pltpu.VMEM((n, half, out_cols), bf16),
            pltpu.VMEM((heads, rows), f32),
            pltpu.VMEM((2, rows, q_cols), f32),
            pltpu.VMEM((2, rows, POOL_CH), f32),
            pltpu.VMEM((2, rows, width), bf16),
            pltpu.VMEM((2, rows, q_cols), bf16),
            pltpu.VMEM((2, WINDOW + rows, kv_cols), bf16),
            pltpu.VMEM((2, TILE + rows, POOL_CH), bf16),
            pltpu.VMEM((2, rows, q_cols + POOL_CH), bf16),
            pltpu.VMEM((POOL_CH, POOL_CH), bf16),
            pltpu.VMEM((2, heads, rows), f32),
            pltpu.VMEM((heads, rows), f32),
            pltpu.VMEM((2 * n, half, out_cols // 2), f32),
            pltpu.VMEM((2 * n, half, out_cols // 2), f32),
            pltpu.VMEM((2 * n, half, out_cols // 2), f32),
            pltpu.VMEM((2 * n, half, out_cols // 2), bf16),
            pltpu.VMEM((n, 2, half, out_cols // 2), bf16),
            pltpu.VMEM((n, half, out_cols), f32),
            pltpu.VMEM((n, half, out_cols), f32),
            pltpu.VMEM((n, half, out_cols), f32),
            dma((2,)),
            dma,
            dma((pieces, n - 1)),
            dma((5 + n - 1,)),
            dma((7,)),
            dma((4,)),
            dma,
            dma,
            dma,
            dma((4,)),
            dma,
            dma((4,)),
            dma((4,)),
            dma((4,)),
            dma,
            dma((2 * n,)),
            dma,
            dma((n,)),
            dma,
            dma((n,)),
            dma,
            dma,
            dma((2,)),
        ],
        compiler_params=pltpu.CompilerParams(
            collective_id=0, has_side_effects=True, vmem_limit_bytes=60 * 1024 * 1024
        ),
    )(
        head_sink_logit,
        tokens[0],
        norm_gain.reshape(1, width),
        query_weight,
        key_matrix,
        value_matrix,
        pool_in_weight,
        pool_mix,
        pool_gain.reshape(-1, 1, POOL_CH),
        attn_out_weight,
        pool_out_weight,
    )
    return mixed[None], logs[None]


def fits(mesh, tokens, query_weight, key_matrix, pool_in_weight, attn_out_weight):
    n, f, c = mesh.shape["sp"], mesh.shape["fs"], mesh.shape["tp"]
    depth = query_weight.shape[0] // n
    rows = tokens.shape[1] // n
    q_cols, kv_cols, pool_cols = (w.shape[1] // c for w in (query_weight, key_matrix, pool_in_weight))
    return (
        n == 4
        and f == 4
        and c == 2
        and tokens.shape[0] == f
        and rows == 4 * WINDOW
        and kv_cols == LANES == 2 * HEAD_SIZE
        and q_cols == 4 * LANES
        and pool_cols == 2 * POOL_CH == q_cols
        and attn_out_weight.shape[1] == n * 4 * LANES
        and attn_out_weight.shape[0] // c == depth == q_cols
    )


def solution(mesh):
    in_specs = (
        P("fs", ("sp", "tp"), None),
        P(),
        P("sp", "tp"),
        P("sp", "tp"),
        P("sp", "tp"),
        P("sp", "tp"),
        P(),
        P(),
        P(),
        P("tp", "sp"),
        P("tp", "sp"),
    )
    out_specs = (P("fs", ("sp", "tp"), None), P("fs", "tp", "sp"))

    def step(*args):
        fused = fits(mesh, args[0], args[2], args[3], args[5], args[9])
        body = functools.partial(fused_local, mesh.shape["sp"]) if fused else local
        mapped = jax.shard_map(body, mesh=mesh, in_specs=in_specs, out_specs=out_specs, check_vma=False)
        return mapped(*args)

    return step
```

time: 79.4 us -> 65.2 us (0.82)
  Pallas kernels: 74.3 us -> 60.4 us
    pallas_call x1, Pallas kernels: 74.3 us -> 60.4 us  [fused_local(): pl.pallas_call(functools.partial(layer_kernel, n), out_shape=(jax.ShapeDt...]
where the time goes in v1:
time: 65.2 us; the launch traced here: 63.9 us
  Pallas kernels  60.4 us (93%)
  local copies, waits for them, and re-layouts  2.92 us (4%)
    pallas_call x1, Pallas kernels, fused_local(): pl.pallas_call(functools.partial(layer_kernel, n), out_shape=(jax.ShapeDt...  60.4 us
    unnamed x4, local copies, waits for them, and re-layouts  2.92 us

profile of v1, /device:TPU:0, one launch (start us, length us, event | category | flops | bytes accessed | tf_op | source)
XLA Modules:
  0.0 63.9 jit_solution(6626099101139494432)
XLA Ops:
  0.6 60.4 %shard_map.122 = (bf16[256,2048]{1,0:T(8,128)(2,1)}, f32[8,512]{1,0:T(8,128)}) custom-call(f32[16]{0:T(128)} %sinks.1, bf16[256,2048]{1,0:T(8,128)(2,1)} %bitcast.5, f32[1,2048]{1,0:T(1,128)} %bitcast.8, bf16[512,512]{1,0:T(8,128)(2,1)} %wq.1, bf16[512,128]{1,0:T(8,128)(2,1)} %wk.1, bf16[512,128]{1,0:T(8,128)(2,1)} %wv.1, bf16[512,512]{1,0:T(8,128)(2,1)} %wp.1, ...), custom_call_target="tpu_custom_call" | custom-call | tf_op jit(solution)/shard_map/pallas_call | solution.py:860
  61.0 0.0 copy-start
  61.0 2.3 %copy.15 = bf16[1,256,2048]{2,1,0:T(8,128)(2,1)} copy(bf16[1,256,2048]{2,1,0:T(8,128)(2,1)} %bitcast.6) | data formatting | bytes 2097152
  63.3 0.0 copy-done
  63.3 0.6 copy.16
Async XLA Ops:
  61.0 2.3 %copy-start = (f32[8,512]{1,0:T(8,128)S(1)}, f32[8,512]{1,0:T(8,128)}, u32[]{:S(2)}) copy-start(f32[8,512]{1,0:T(8,128)} %get-tuple-element.5) | copy-start | bytes 49156

commit v2 on v1

--- a/solution.py
+++ b/solution.py
@@ -224,6 +224,11 @@
     got_n,
     y_part,
     y_got,
+    keep_m,
+    send_m,
+    got_m,
+    y_part_m,
+    y_got_m,
     mine,
     sent,
     got,
@@ -262,8 +267,9 @@
     q_cols = wq.shape[1] // 2
     group = q_cols // HEAD_SIZE
     out_cols = wao.shape[1]
-    n_in = held.shape[1]
+    n_in = held.shape[1] + 1
     n_pieces = n_in + OUT_CUTS
+    n_units = n_pieces - 1
     chunk = half // 4
     blocks = rows // WINDOW
     y, x = f // 2, lax.rem(f, 2)
@@ -299,14 +305,29 @@
         first_loads.append(pltpu.make_async_copy(at_cols(wq, i), held.at[me, 1 + i], load_sem.at[0]))
     for i in range(2):
         first_loads.append(pltpu.make_async_copy(at_cols(wp, i), held.at[me, 3 + i], load_sem.at[0]))
+    out_loads = []
+    for i in range(out_cols // LANES):
+        for side, w in enumerate((wao, wpo)):
+            to = wout.at[me, i, pl.ds(side * part_rows, part_rows)]
+            out_loads.append(pltpu.make_async_copy(w.at[y_rows, pl.ds(i * LANES, LANES)], to, load_sem.at[1]))
     late_loads = [
-        pltpu.make_async_copy(wao.at[y_rows], wout.at[me, pl.ds(0, part_rows)], load_sem.at[1]),
-        pltpu.make_async_copy(wpo.at[y_rows], wout.at[me, pl.ds(part_rows, part_rows)], load_sem.at[2]),
         pltpu.make_async_copy(mix.at[pool_index], mix_own, load_sem.at[3]),
         pltpu.make_async_copy(pool_gain, pgain_v, load_sem.at[4]),
         pltpu.make_async_copy(sinks, sink_v, load_sem.at[5]),
     ]
     gain_load = pltpu.make_async_copy(gain, gain_v, load_sem.at[6])
+    barrier = pltpu.get_barrier_semaphore()
+    for peer in ({"tp": 1 - c}, {"fs": beside}, {"fs": across}, {"fs": across, "tp": 1 - c}):
+        pl.semaphore_signal(barrier, inc=1, device_id=peer, device_id_type=MESH_ID)
+
+    @pl.when(has_up)
+    def _():
+        pl.semaphore_signal(barrier, inc=1, device_id={"sp": up}, device_id_type=MESH_ID)
+
+    @pl.when(has_down)
+    def _():
+        pl.semaphore_signal(barrier, inc=1, device_id={"sp": down}, device_id_type=MESH_ID)
+
     for cp in first_loads[:2]:
         cp.start()
     tok_load(norm_order[0]).start()
@@ -315,29 +336,20 @@
         cp.start()
     for i in norm_order[1:]:
         tok_load(i).start()
-    for cp in late_loads:
+    for cp in out_loads + late_loads:
         cp.start()
-
-    barrier = pltpu.get_barrier_semaphore()
-    for peer in ({"tp": 1 - c}, {"fs": beside}, {"fs": across}, {"fs": across, "tp": 1 - c}):
-        pl.semaphore_signal(barrier, inc=1, device_id=peer, device_id_type=MESH_ID)
-
-    @pl.when(has_up)
-    def _():
-        pl.semaphore_signal(barrier, inc=1, device_id={"sp": up}, device_id_type=MESH_ID)
-
-    @pl.when(has_down)
-    def _():
-        pl.semaphore_signal(barrier, inc=1, device_id={"sp": down}, device_id_type=MESH_ID)
 
     def remote(src, dst, send, recv, to):
         return pltpu.make_async_remote_copy(src, dst, send, recv, device_id=to, device_id_type=MESH_ID)
 
     def piece(s, j, part):
+        if s < n_in - 2:
+            return held.at[j, s, pl.ds(pl.multiple_of(part * part_rows, part_rows), part_rows)]
         if s < n_in:
-            return held.at[j, s, pl.ds(pl.multiple_of(part * part_rows, part_rows), part_rows)]
-        size = part_rows // OUT_CUTS
-        return wout.at[j, pl.ds(pl.multiple_of(part * part_rows + (s - n_in) * size, size), size)]
+            size = part_rows // 2
+            return held.at[j, n_in - 2, pl.ds(pl.multiple_of(part * part_rows + (s - n_in + 2) * size, size), size)]
+        block, side = divmod(s - n_in, 2)
+        return wout.at[j, 2 * part + block, pl.ds(side * part_rows, part_rows)]
 
     def bulk(count):
         return nrm.at[0, pl.ds(0, count * part_rows * LANES // width)]
@@ -357,7 +369,7 @@
     def x_group(s, k):
         if s >= n_in:
             return 5 + k
-        return 0 if s == 0 else 1 + 2 * ((s - 1) // 2) + k // (n - 2)
+        return 0 if s == 0 else 1 + 2 * min((s - 1) // 2, 1) + k // (n - 2)
 
     def x_hop(s, k):
         block = piece(s, shard[k], x)
@@ -569,36 +581,51 @@
         return remote(logs.at[1], logs_got, log_send, log_recv, {"fs": across})
 
     order = [me] + shard
-    wide = out_cols // 2
-
-    def sum_n(part, i):
-        u = i * 2 + part
-        return remote(send_n.at[u], got_n.at[u], sumn_send, sumn_recv.at[u], {"tp": 1 - c})
+
+    def unit(part, i, g):
+        return part if i == 0 else 4 * (i - 1) + 2 * g + part
+
+    def sum_n(part, i, g):
+        u = unit(part, i, g)
+        a, b = (send_n, got_n) if i == 0 else (send_m, got_m)
+        return remote(a.at[u], b.at[u], sumn_send.at[min(i, 1)], sumn_recv.at[u + 2 * min(i, 1)], {"tp": 1 - c})
+
+    def all_cols(j):
+        return jnp.concatenate([wout[j, i] for i in range(out_cols // LANES)], axis=1)
 
     def sum_o(i):
         return remote(sent.at[i], got.at[i], sumo_send, sumo_recv.at[i], {"tp": 1 - c})
 
-    def y_sum(part, i):
-        return remote(
-            y_part.at[i * 2 + part], y_got.at[i, c], yp_send, yp_recv.at[i], {"fs": across, "tp": part}
-        )
-
-    def out_far(part, i):
-        u = i * 2 + part
-        acc = jnp.dot(mixed[1, part * half : (part + 1) * half, :], wout[order[i]], preferred_element_type=f32)
-        left, right = acc[:, :wide], acc[:, wide:]
-        keep_n[u] = jnp.where(c == 0, left, right)
-        send_n[u] = jnp.where(c == 0, right, left)
-        sum_n(part, i).start()
-
-    def pass_far(part, i):
-        u = i * 2 + part
-        sum_n(part, i).wait_recv()
-        y_part[u] = (keep_n[u] + got_n[u]).astype(bf16)
-        y_sum(part, i).start()
+    def y_sum(part, i, g):
+        u = unit(part, i, g)
+        src, dst = (y_part.at[u], y_got.at[c]) if i == 0 else (y_part_m.at[u], y_got_m.at[i - 1, g, c])
+        return remote(src, dst, yp_send.at[min(i, 1)], yp_recv.at[i], {"fs": across, "tp": part})
+
+    def out_far(part, i, g):
+        u = unit(part, i, g)
+        j = order[i]
+        keep, send = (keep_n, send_n) if i == 0 else (keep_m, send_m)
+        if i == 0:
+            w = all_cols(j)
+        else:
+            first = 2 * (x if g == 0 else 1 - x)
+            w = jnp.concatenate([wout[j, first], wout[j, first + 1]], axis=1)
+        acc = jnp.dot(mixed[1, part * half : (part + 1) * half, :], w, preferred_element_type=f32)
+        across_cols = acc.shape[1] // 2
+        left, right = acc[:, :across_cols], acc[:, across_cols:]
+        keep[u] = jnp.where(c == 0, left, right)
+        send[u] = jnp.where(c == 0, right, left).astype(bf16)
+        sum_n(part, i, g).start()
+
+    def pass_far(part, i, g):
+        u = unit(part, i, g)
+        keep, there, to = (keep_n, got_n, y_part) if i == 0 else (keep_m, got_m, y_part_m)
+        sum_n(part, i, g).wait_recv()
+        to[u] = (keep[u] + there[u].astype(f32)).astype(bf16)
+        y_sum(part, i, g).start()
 
     def out_own(i):
-        acc = jnp.dot(mixed[0], wout[order[i]], preferred_element_type=f32)
+        acc = jnp.dot(mixed[0], all_cols(order[i]), preferred_element_type=f32)
         low, high = acc[:half], acc[half:]
         mine[i] = jnp.where(c == 0, low, high)
         sent[i] = jnp.where(c == 0, high, low)
@@ -606,8 +633,16 @@
 
     def finish(i):
         sum_o(i).wait_recv()
-        got_all(y_got.at[i], yp_recv.at[i])
-        there = jnp.concatenate([y_got[i, 0], y_got[i, 1]], axis=1).astype(f32)
+        if i == 0:
+            got_all(y_got, yp_recv.at[i])
+            there = jnp.concatenate([y_got[0], y_got[1]], axis=1).astype(f32)
+        else:
+            got_all(y_got_m.at[i - 1], yp_recv.at[i])
+            near = [y_got_m[i - 1, 0, 0], y_got_m[i - 1, 0, 1]]
+            other = [y_got_m[i - 1, 1, 0], y_got_m[i - 1, 1, 1]]
+            there = jnp.where(
+                x == 0, jnp.concatenate(near + other, axis=1), jnp.concatenate(other + near, axis=1)
+            ).astype(f32)
         out_v[i] = (mine[i] + got[i] + there).astype(bf16)
         out_copy(i).start()
 
@@ -634,11 +669,11 @@
             @pl.when(me == z)
             def _():
                 if z < n - 1:
-                    sent_all(bulk(n_pieces * (z + 1)), z_send.at[0])
+                    sent_all(bulk(n_units * (z + 1)), z_send.at[0])
                 if z:
-                    sent_all(bulk(n_pieces * (n - z)), z_send.at[1])
-
-        sent_all(bulk(n_pieces * (n - 1)), x_send)
+                    sent_all(bulk(n_units * (n - z)), z_send.at[1])
+
+        sent_all(bulk(n_units * (n - 1)), x_send)
         for sem in (tok_send, ytok_send, fwd_send):
             sent_all(nrm.at[0, pl.ds(0, half)], sem)
 
@@ -658,175 +693,198 @@
         fwd(i).wait_recv()
 
     def late_wait():
+        pltpu.make_async_copy(wout.at[me], wout.at[me], load_sem.at[1]).wait()
         for cp in late_loads:
             cp.wait()
 
     W = WINDOW
     send_end(1)
     send_inner(1)
+    send_inner(0)
+    send_inner(4)
+    send_end(0)
     norm(2)
     norm(0)
     norm(1)
     norm(3)
-    send_end(2)
+    send_end(5)
     send_inner(2)
-    send_inner(0)
-    send_end(0)
+    inner_slot(1, 1)
+    send_end(4)
     inner_slot(1, 0)
-    inner_slot(1, 1)
-    send_end(3)
-    inner_slot(2, 0)
-    send_end(4)
-    end_slot(1, 0)
-    inner_slot(2, 1)
-    end_slot(2, 0)
-    own_tokens()
-    end_slot(0, 0)
-    end_slot(1, 1)
-    end_slot(2, 1)
-    inner_slot(0, 1)
-    end_slot(0, 1)
-    inner_slot(0, 0)
-    end_slot(1, 2)
-    inner_slot(1, 2)
-    y_service(0)
     late_wait()
     send_end(8)
+    inner_slot(0, 0)
+    send_end(2)
+    end_slot(1, 0)
+    inner_slot(0, 1)
+    send_inner(3)
+    own_tokens()
+    send_inner(5)
+    end_slot(0, 0)
+    send_end(3)
+    inner_slot(1, 2)
+    inner_slot(0, 2)
+    end_slot(4, 0)
+    end_slot(2, 0)
+    end_slot(1, 1)
+    end_slot(0, 1)
+    end_slot(3, 0)
+    inner_slot(2, 0)
+    inner_slot(2, 1)
+    inner_slot(4, 1)
+    end_slot(5, 0)
+    inner_slot(4, 0)
+    send_end(7)
+    inner_slot(2, 2)
+    end_slot(1, 2)
+    end_slot(0, 2)
+    end_slot(2, 1)
+    inner_slot(5, 0)
+    inner_slot(3, 0)
+    inner_slot(5, 1)
+    y_service(1)
+    inner_slot(3, 1)
+    send_end(9)
+    end_slot(4, 1)
+    y_service(0)
+    send_end(6)
+    inner_slot(4, 2)
+    inner_slot(5, 2)
     end_slot(2, 2)
-    inner_slot(2, 2)
-    inner_slot(0, 2)
-    send_inner(4)
-    send_inner(3)
-    y_service(1)
+    ready([0], range(n - 1))
+    project_kv(0, 0, half)
+    end_slot(5, 1)
+    arrived(1)
+    arrived(0)
+    project_kv(1, W, 2 * W)
+    inner_slot(3, 2)
+    send_inner(7)
+    end_slot(3, 1)
+    send_inner(8)
     ready([1, 2], range(n - 2))
     begin_q(0, half, half)
-    end_slot(0, 2)
-    send_end(6)
-    arrived(0)
-    inner_slot(4, 0)
-    inner_slot(4, 1)
-    inner_slot(3, 1)
-    inner_slot(3, 0)
-    end_slot(4, 0)
+    y_service(2)
     begin_q(0, 0, half)
+    end_slot(4, 2)
+    send_inner(6)
+    begin_q(1, W, 2 * W)
+    project_kv(0, half, half)
+    end_slot(5, 2)
     ready([1, 2], [n - 2])
-    end_q(0, 0, half)
-    end_slot(3, 0)
-    inner_slot(4, 2)
-    arrived(1)
-    begin_q(1, W, 2 * W)
-    ready([0], range(n - 1))
-    project_kv(0, 0, half)
     end_q(0, half, half)
-    end_slot(4, 1)
-    send_end(5)
-    inner_slot(3, 2)
-    send_inner(5)
-    project_kv(0, half, half)
+    attend(0, 3)
+    end_slot(3, 2)
     attend(0, 2)
-    y_service(2)
-    end_slot(3, 1)
-    send_inner(6)
-    send_end(7)
-    send_inner(8)
-    attend(0, 1)
-    project_kv(1, W, 2 * W)
-    end_slot(4, 2)
-    attend(0, 3)
+    send_inner(9)
+    inner_slot(7, 1)
     arrived(2)
     project_kv(1, 3 * W, W)
     send_halo(halo_kv, 1)
-    send_inner(7)
-    inner_slot(5, 1)
-    inner_slot(5, 0)
-    end_slot(3, 2)
+    inner_slot(7, 0)
     end_q(1, W, 2 * W)
     attend(1, 2)
-    ready([3, 4], range(n - 2))
-    begin_pool(0, half, half)
-    end_slot(5, 0)
+    end_slot(7, 0)
+    inner_slot(8, 1)
     y_service(3)
     begin_q(1, 3 * W, W)
     end_q(1, 3 * W, W)
     attend(1, 3)
-    end_slot(6, 0)
+    ready([3, 4], range(n - 2))
     begin_pool(1, half - TILE, half + TILE)
     ready([3, 4], [n - 2])
     end_pool(1, half - TILE, half + TILE)
+    pool(1, 1)
+    out_far(1, 0, 0)
     send_halo(halo_pool, 1)
     inner_slot(6, 0)
-    pool(1, 1)
-    out_far(1, 0)
-    end_pool(0, half, half)
-    send_halo(halo_pool, 0)
-    inner_slot(7, 0)
-    send_halo(halo_kv, 0)
+    end_slot(6, 0)
+    end_q(0, 0, half)
+    arrived(3)
+    project_q(1, 0, W)
     inner_slot(8, 0)
+    end_slot(8, 0)
+    inner_slot(9, 0)
+    end_slot(9, 0)
+    out_far(1, 1, 0)
     inner_slot(6, 1)
-    end_slot(8, 0)
-    inner_slot(7, 1)
-    inner_slot(8, 1)
-    arrived(3)
     project_kv(1, 0, W)
     attend(1, 1)
+    pass_far(1, 0, 0)
     wait_halo(halo_kv, 1)
-    project_q(1, 0, W)
     attend(1, 0)
     send_log()
-    pass_far(1, 0)
-    inner_slot(5, 2)
-    end_slot(7, 0)
+    pass_far(1, 1, 0)
+    send_halo(halo_kv, 0)
+    inner_slot(9, 1)
+    end_slot(7, 1)
     project_pool(1, 0, half - TILE)
     wait_halo(halo_pool, 1)
     pool(1, 0)
-    out_far(0, 0)
-    end_slot(5, 1)
+    out_far(0, 0, 0)
+    begin_pool(0, half, half)
+    end_pool(0, half, half)
+    send_halo(halo_pool, 0)
+    end_slot(6, 1)
+    out_far(0, 1, 0)
+    inner_slot(7, 2)
+    inner_slot(6, 2)
     begin_pool(0, 0, half)
     end_pool(0, 0, half)
     pool(0, 1)
+    end_slot(8, 1)
+    inner_slot(8, 2)
+    pass_far(0, 0, 0)
+    attend(0, 1)
+    pass_far(0, 1, 0)
+    inner_slot(9, 2)
+    end_slot(9, 1)
+    out_far(1, 2, 0)
+    ready_out(0)
+    out_far(1, 1, 1)
+    out_far(0, 1, 1)
+    out_far(0, 2, 0)
     wait_halo(halo_pool, 0)
     pool(0, 0)
-    inner_slot(7, 2)
-    end_slot(6, 1)
-    inner_slot(6, 2)
-    ready_out(0)
-    out_far(0, 1)
-    inner_slot(8, 2)
-    end_slot(7, 1)
-    pass_far(0, 0)
-    out_far(1, 1)
     wait_halo(halo_kv, 0)
     attend(0, 0)
     out_own(0)
-    end_slot(8, 1)
+    pass_far(1, 1, 1)
+    end_slot(7, 2)
+    write_log()
+    pass_far(0, 1, 1)
+    pass_far(1, 2, 0)
+    pass_far(0, 2, 0)
     out_own(1)
-    pass_far(0, 1)
-    pass_far(1, 1)
-    end_slot(5, 2)
-    end_slot(7, 2)
+    end_slot(6, 2)
+    end_slot(8, 2)
+    ready_out(1)
+    out_far(0, 2, 1)
+    out_far(1, 2, 1)
     finish(0)
-    ready_out(1)
-    out_far(1, 2)
-    out_far(0, 2)
-    end_slot(6, 2)
+    end_slot(9, 2)
+    out_far(0, 3, 0)
+    out_far(1, 3, 0)
     out_own(2)
-    end_slot(8, 2)
-    drain()
-    write_log()
-    pass_far(1, 2)
-    pass_far(0, 2)
+    pass_far(0, 2, 1)
+    pass_far(1, 2, 1)
+    pass_far(0, 3, 0)
+    pass_far(1, 3, 0)
     finish(1)
     ready_out(2)
-    out_far(0, 3)
-    out_far(1, 3)
+    out_far(1, 3, 1)
+    out_far(0, 3, 1)
     out_own(3)
-    pass_far(0, 3)
-    pass_far(1, 3)
+    pass_far(1, 3, 1)
+    pass_far(0, 3, 1)
+    drain()
     finish(2)
     finish(3)
-    sent_all(send_n, sumn_send)
+    sent_all(send_n, sumn_send.at[0])
+    sent_all(send_m, sumn_send.at[1])
     sent_all(sent, sumo_send)
-    sent_all(y_part, yp_send)
+    sent_all(y_part, yp_send.at[0])
+    sent_all(y_part_m, yp_send.at[1])
     pltpu.make_async_copy(out, out, out_sem.at[0]).wait()
     log_copy.wait()
 
@@ -853,7 +911,7 @@
     q_cols = q_all // 2
     out_cols = attn_out_weight.shape[1]
     n_in = 1 + 2 * (q_cols // LANES)
-    pieces = n_in + OUT_CUTS
+    pieces = n_in + 1 + OUT_CUTS
     bf16, f32 = jnp.bfloat16, jnp.float32
     dma = pltpu.SemaphoreType.DMA
     hbm = pl.BlockSpec(memory_space=pl.ANY)
@@ -867,7 +925,7 @@
         out_specs=(hbm, hbm),
         scratch_shapes=[
             pltpu.VMEM((n, n_in, depth, LANES), bf16),
-            pltpu.VMEM((n, depth, out_cols), bf16),
+            pltpu.VMEM((n, out_cols // LANES, depth, LANES), bf16),
             pltpu.VMEM((2, depth, kv_cols), bf16),
             pltpu.VMEM((half, width), bf16),
             pltpu.VMEM((1, width), f32),
@@ -885,11 +943,16 @@
             pltpu.VMEM((POOL_CH, POOL_CH), bf16),
             pltpu.VMEM((2, heads, rows), f32),
             pltpu.VMEM((heads, rows), f32),
-            pltpu.VMEM((2 * n, half, out_cols // 2), f32),
-            pltpu.VMEM((2 * n, half, out_cols // 2), f32),
-            pltpu.VMEM((2 * n, half, out_cols // 2), f32),
-            pltpu.VMEM((2 * n, half, out_cols // 2), bf16),
-            pltpu.VMEM((n, 2, half, out_cols // 2), bf16),
+            pltpu.VMEM((2, half, out_cols // 2), f32),
+            pltpu.VMEM((2, half, out_cols // 2), bf16),
+            pltpu.VMEM((2, half, out_cols // 2), bf16),
+            pltpu.VMEM((2, half, out_cols // 2), bf16),
+            pltpu.VMEM((2, half, out_cols // 2), bf16),
+            pltpu.VMEM((4 * (n - 1), half, out_cols // 4), f32),
+            pltpu.VMEM((4 * (n - 1), half, out_cols // 4), bf16),
+            pltpu.VMEM((4 * (n - 1), half, out_cols // 4), bf16),
+            pltpu.VMEM((4 * (n - 1), half, out_cols // 4), bf16),
+            pltpu.VMEM((n - 1, 2, 2, half, out_cols // 4), bf16),
             pltpu.VMEM((n, half, out_cols), f32),
             pltpu.VMEM((n, half, out_cols), f32),
             pltpu.VMEM((n, half, out_cols), f32),
@@ -907,11 +970,11 @@
             dma((4,)),
             dma((4,)),
             dma((4,)),
-            dma,
-            dma((2 * n,)),
+            dma((2,)),
+            dma((2 + 4 * (n - 1),)),
             dma,
             dma((n,)),
-            dma,
+            dma((2,)),
             dma((n,)),
             dma,
             dma,

time: 65.2 us -> 64.4 us (0.988); the launches traced: 63.9 us -> 64.2 us
  no operation moved by 1% of the time
where the time goes in v2:
time: 64.4 us; the launch traced here: 64.2 us
  Pallas kernels  60.6 us (94%)
  local copies, waits for them, and re-layouts  2.92 us (5%)
  between operations  0.65 us (1%)
    pallas_call x1, Pallas kernels, fused_local(): pl.pallas_call(functools.partial(layer_kernel, n), out_shape=(jax.ShapeDt...  60.6 us
    unnamed x4, local copies, waits for them, and re-layouts  2.92 us

profile of v2, /device:TPU:0, one launch (start us, length us, event | category | flops | bytes accessed | tf_op | source)
XLA Modules:
  0.0 64.2 jit_solution(16882194336036591055)
XLA Ops:
  0.6 60.6 %shard_map.122 = (bf16[256,2048]{1,0:T(8,128)(2,1)}, f32[8,512]{1,0:T(8,128)}) custom-call(f32[16]{0:T(128)} %sinks.1, bf16[256,2048]{1,0:T(8,128)(2,1)} %bitcast.5, f32[1,2048]{1,0:T(1,128)} %bitcast.8, bf16[512,512]{1,0:T(8,128)(2,1)} %wq.1, bf16[512,128]{1,0:T(8,128)(2,1)} %wk.1, bf16[512,128]{1,0:T(8,128)(2,1)} %wv.1, bf16[512,512]{1,0:T(8,128)(2,1)} %wp.1, ...), custom_call_target="tpu_custom_call" | custom-call | tf_op jit(solution)/shard_map/pallas_call | solution.py:918
  61.3 0.0 copy-start
  61.3 2.3 %copy.15 = bf16[1,256,2048]{2,1,0:T(8,128)(2,1)} copy(bf16[1,256,2048]{2,1,0:T(8,128)(2,1)} %bitcast.6) | data formatting | bytes 2097152
  63.6 0.0 copy-done
  63.6 0.6 copy.16
Async XLA Ops:
  61.3 2.3 %copy-start = (f32[8,512]{1,0:T(8,128)S(1)}, f32[8,512]{1,0:T(8,128)}, u32[]{:S(2)}) copy-start(f32[8,512]{1,0:T(8,128)} %get-tuple-element.5) | copy-start | bytes 49156

commit v3 on v2

--- a/solution.py
+++ b/solution.py
@@ -628,7 +628,7 @@
         acc = jnp.dot(mixed[0], all_cols(order[i]), preferred_element_type=f32)
         low, high = acc[:half], acc[half:]
         mine[i] = jnp.where(c == 0, low, high)
-        sent[i] = jnp.where(c == 0, high, low)
+        sent[i] = jnp.where(c == 0, high, low).astype(bf16)
         sum_o(i).start()
 
     def finish(i):
@@ -643,7 +643,7 @@
             there = jnp.where(
                 x == 0, jnp.concatenate(near + other, axis=1), jnp.concatenate(other + near, axis=1)
             ).astype(f32)
-        out_v[i] = (mine[i] + got[i] + there).astype(bf16)
+        out_v[i] = (mine[i] + got[i].astype(f32) + there).astype(bf16)
         out_copy(i).start()
 
     def out_copy(i):
@@ -699,94 +699,95 @@
 
     W = WINDOW
     send_end(1)
+    send_end(2)
     send_inner(1)
-    send_inner(0)
-    send_inner(4)
-    send_end(0)
     norm(2)
     norm(0)
     norm(1)
     norm(3)
-    send_end(5)
     send_inner(2)
+    send_inner(0)
+    send_end(0)
+    end_slot(1, 0)
+    end_slot(2, 0)
+    inner_slot(1, 0)
     inner_slot(1, 1)
-    send_end(4)
-    inner_slot(1, 0)
+    own_tokens()
+    end_slot(0, 0)
+    inner_slot(2, 1)
+    inner_slot(2, 0)
+    end_slot(1, 1)
+    inner_slot(0, 1)
+    inner_slot(0, 0)
+    send_end(3)
+    inner_slot(1, 2)
+    end_slot(2, 1)
+    inner_slot(2, 2)
     late_wait()
     send_end(8)
-    inner_slot(0, 0)
-    send_end(2)
-    end_slot(1, 0)
-    inner_slot(0, 1)
+    inner_slot(0, 2)
+    send_end(4)
+    send_inner(4)
+    send_end(5)
+    send_inner(5)
+    end_slot(0, 1)
     send_inner(3)
-    own_tokens()
-    send_inner(5)
-    end_slot(0, 0)
-    send_end(3)
-    inner_slot(1, 2)
-    inner_slot(0, 2)
+    end_slot(1, 2)
+    end_slot(2, 2)
+    ready([1, 2], range(n - 2))
+    begin_q(0, half, half)
+    inner_slot(4, 1)
+    inner_slot(4, 0)
+    end_slot(0, 2)
+    inner_slot(5, 1)
+    send_end(6)
     end_slot(4, 0)
-    end_slot(2, 0)
-    end_slot(1, 1)
-    end_slot(0, 1)
-    end_slot(3, 0)
-    inner_slot(2, 0)
-    inner_slot(2, 1)
-    inner_slot(4, 1)
-    end_slot(5, 0)
-    inner_slot(4, 0)
-    send_end(7)
-    inner_slot(2, 2)
-    end_slot(1, 2)
-    end_slot(0, 2)
-    end_slot(2, 1)
     inner_slot(5, 0)
     inner_slot(3, 0)
-    inner_slot(5, 1)
-    y_service(1)
+    end_slot(5, 0)
     inner_slot(3, 1)
+    inner_slot(4, 2)
+    begin_q(0, 0, half)
+    ready([1, 2], [n - 2])
+    end_q(0, 0, half)
+    y_service(0)
     send_end(9)
-    end_slot(4, 1)
-    y_service(0)
-    send_end(6)
-    inner_slot(4, 2)
+    end_slot(3, 0)
     inner_slot(5, 2)
-    end_slot(2, 2)
+    end_q(0, half, half)
     ready([0], range(n - 1))
     project_kv(0, 0, half)
+    inner_slot(3, 2)
+    send_inner(6)
+    end_slot(4, 1)
+    y_service(1)
     end_slot(5, 1)
+    attend(0, 1)
+    y_service(2)
+    project_kv(0, half, half)
+    end_slot(3, 1)
+    attend(0, 3)
+    send_inner(8)
+    send_inner(9)
+    end_slot(4, 2)
+    attend(0, 2)
+    end_slot(5, 2)
+    send_inner(7)
+    arrived(0)
     arrived(1)
-    arrived(0)
-    project_kv(1, W, 2 * W)
-    inner_slot(3, 2)
-    send_inner(7)
-    end_slot(3, 1)
-    send_inner(8)
-    ready([1, 2], range(n - 2))
-    begin_q(0, half, half)
-    y_service(2)
-    begin_q(0, 0, half)
-    end_slot(4, 2)
-    send_inner(6)
     begin_q(1, W, 2 * W)
-    project_kv(0, half, half)
-    end_slot(5, 2)
-    ready([1, 2], [n - 2])
-    end_q(0, half, half)
-    attend(0, 3)
-    end_slot(3, 2)
-    attend(0, 2)
-    send_inner(9)
-    inner_slot(7, 1)
     arrived(2)
     project_kv(1, 3 * W, W)
     send_halo(halo_kv, 1)
-    inner_slot(7, 0)
+    send_end(7)
+    end_slot(3, 2)
+    inner_slot(6, 0)
+    inner_slot(6, 1)
     end_q(1, W, 2 * W)
+    project_kv(1, W, 2 * W)
     attend(1, 2)
-    end_slot(7, 0)
-    inner_slot(8, 1)
     y_service(3)
+    end_slot(6, 0)
     begin_q(1, 3 * W, W)
     end_q(1, 3 * W, W)
     attend(1, 3)
@@ -796,89 +797,88 @@
     end_pool(1, half - TILE, half + TILE)
     pool(1, 1)
     out_far(1, 0, 0)
+    end_slot(8, 0)
     send_halo(halo_pool, 1)
-    inner_slot(6, 0)
-    end_slot(6, 0)
-    end_q(0, 0, half)
+    inner_slot(7, 0)
+    end_slot(9, 0)
     arrived(3)
-    project_q(1, 0, W)
-    inner_slot(8, 0)
-    end_slot(8, 0)
-    inner_slot(9, 0)
-    end_slot(9, 0)
-    out_far(1, 1, 0)
-    inner_slot(6, 1)
     project_kv(1, 0, W)
     attend(1, 1)
+    inner_slot(8, 0)
+    inner_slot(9, 0)
+    end_slot(7, 0)
+    out_far(1, 1, 0)
+    inner_slot(7, 1)
+    inner_slot(8, 1)
+    project_pool(1, 0, half - TILE)
+    project_q(1, 0, W)
     pass_far(1, 0, 0)
+    inner_slot(9, 1)
     wait_halo(halo_kv, 1)
     attend(1, 0)
-    send_log()
-    pass_far(1, 1, 0)
-    send_halo(halo_kv, 0)
-    inner_slot(9, 1)
-    end_slot(7, 1)
-    project_pool(1, 0, half - TILE)
     wait_halo(halo_pool, 1)
     pool(1, 0)
     out_far(0, 0, 0)
+    end_slot(6, 1)
+    pass_far(1, 1, 0)
+    out_far(0, 1, 0)
     begin_pool(0, half, half)
     end_pool(0, half, half)
     send_halo(halo_pool, 0)
-    end_slot(6, 1)
-    out_far(0, 1, 0)
+    send_halo(halo_kv, 0)
     inner_slot(7, 2)
     inner_slot(6, 2)
+    end_slot(7, 1)
     begin_pool(0, 0, half)
     end_pool(0, 0, half)
     pool(0, 1)
+    ready_out(0)
+    out_far(0, 1, 1)
+    out_far(1, 1, 1)
+    pass_far(0, 0, 0)
+    inner_slot(8, 2)
+    pass_far(0, 1, 0)
     end_slot(8, 1)
-    inner_slot(8, 2)
-    pass_far(0, 0, 0)
-    attend(0, 1)
-    pass_far(0, 1, 0)
-    inner_slot(9, 2)
     end_slot(9, 1)
     out_far(1, 2, 0)
-    ready_out(0)
-    out_far(1, 1, 1)
-    out_far(0, 1, 1)
-    out_far(0, 2, 0)
     wait_halo(halo_pool, 0)
     pool(0, 0)
+    out_far(0, 2, 0)
+    inner_slot(9, 2)
     wait_halo(halo_kv, 0)
     attend(0, 0)
     out_own(0)
     pass_far(1, 1, 1)
+    pass_far(0, 1, 1)
     end_slot(7, 2)
-    write_log()
-    pass_far(0, 1, 1)
+    out_own(1)
     pass_far(1, 2, 0)
     pass_far(0, 2, 0)
-    out_own(1)
     end_slot(6, 2)
+    ready_out(1)
+    out_far(1, 2, 1)
+    out_far(0, 2, 1)
+    out_own(2)
     end_slot(8, 2)
-    ready_out(1)
-    out_far(0, 2, 1)
-    out_far(1, 2, 1)
     finish(0)
     end_slot(9, 2)
+    out_far(1, 3, 0)
     out_far(0, 3, 0)
-    out_far(1, 3, 0)
-    out_own(2)
+    pass_far(1, 2, 1)
     pass_far(0, 2, 1)
-    pass_far(1, 2, 1)
+    finish(1)
+    drain()
+    pass_far(1, 3, 0)
+    send_log()
     pass_far(0, 3, 0)
-    pass_far(1, 3, 0)
-    finish(1)
     ready_out(2)
     out_far(1, 3, 1)
     out_far(0, 3, 1)
     out_own(3)
     pass_far(1, 3, 1)
     pass_far(0, 3, 1)
-    drain()
     finish(2)
+    write_log()
     finish(3)
     sent_all(send_n, sumn_send.at[0])
     sent_all(send_m, sumn_send.at[1])
@@ -954,8 +954,8 @@
             pltpu.VMEM((4 * (n - 1), half, out_cols // 4), bf16),
             pltpu.VMEM((n - 1, 2, 2, half, out_cols // 4), bf16),
             pltpu.VMEM((n, half, out_cols), f32),
-            pltpu.VMEM((n, half, out_cols), f32),
-            pltpu.VMEM((n, half, out_cols), f32),
+            pltpu.VMEM((n, half, out_cols), bf16),
+            pltpu.VMEM((n, half, out_cols), bf16),
             dma((2,)),
             dma,
             dma((pieces, n - 1)),

time: 64.4 us -> 64.2 us (level)
  no operation moved by 1% of the time
where the time goes in v3:
time: 64.2 us; the launch traced here: 64.1 us
  Pallas kernels  60.5 us (94%)
  local copies, waits for them, and re-layouts  2.92 us (5%)
  between operations  0.65 us (1%)
    pallas_call x1, Pallas kernels, fused_local(): pl.pallas_call(functools.partial(layer_kernel, n), out_shape=(jax.ShapeDt...  60.5 us
    unnamed x4, local copies, waits for them, and re-layouts  2.92 us

profile of v3, /device:TPU:0, one launch (start us, length us, event | category | flops | bytes accessed | tf_op | source)
XLA Modules:
  0.0 64.1 jit_solution(3388570895336167454)
XLA Ops:
  0.6 60.5 %shard_map.122 = (bf16[256,2048]{1,0:T(8,128)(2,1)}, f32[8,512]{1,0:T(8,128)}) custom-call(f32[16]{0:T(128)} %sinks.1, bf16[256,2048]{1,0:T(8,128)(2,1)} %bitcast.5, f32[1,2048]{1,0:T(1,128)} %bitcast.8, bf16[512,512]{1,0:T(8,128)(2,1)} %wq.1, bf16[512,128]{1,0:T(8,128)(2,1)} %wk.1, bf16[512,128]{1,0:T(8,128)(2,1)} %wv.1, bf16[512,512]{1,0:T(8,128)(2,1)} %wp.1, ...), custom_call_target="tpu_custom_call" | custom-call | tf_op jit(solution)/shard_map/pallas_call | solution.py:918
  61.2 0.0 copy-start
  61.2 2.3 %copy.15 = bf16[1,256,2048]{2,1,0:T(8,128)(2,1)} copy(bf16[1,256,2048]{2,1,0:T(8,128)(2,1)} %bitcast.6) | data formatting | bytes 2097152
  63.5 0.0 copy-done
  63.5 0.6 copy.16
Async XLA Ops:
  61.2 2.3 %copy-start = (f32[8,512]{1,0:T(8,128)S(1)}, f32[8,512]{1,0:T(8,128)}, u32[]{:S(2)}) copy-start(f32[8,512]{1,0:T(8,128)} %get-tuple-element.5) | copy-start | bytes 49156
